TPU v7x, 512 devices: a whole 4x4x16 slice. The times are simulated.
512 devices in a mesh: ep: 32 (over z, core), tp: 16 (over y, x).
Axes of the slice: x: 4, y: 4, z: 16, core: 2. Of those that a mesh axis runs over, the one named last changes fastest.
Arguments:
- receptance: bfloat16 [8192, 2048], P('ep', 'tp'), may hold values from -6 to 6
- key_tensor: bfloat16 [8192, 2048], P('ep', 'tp'), may hold values from -6 to 6
- value_tensor: bfloat16 [8192, 2048], P('ep', 'tp'), may hold values from -6 to 6
- decay_data_input: bfloat16 [8192, 2048], P('ep', 'tp'), may hold values from -4 to 4
- correction_rate_input: bfloat16 [8192, 2048], P('ep', 'tp'), may hold values from -16 to 6
- mixer_output_gate: bfloat16 [8192, 2048], P('ep', 'tp'), may hold values from -6 to 6
- decay_channel_offset: float32 [2048], P('tp'), may hold values from -16 to -3
- head_norm_gain: float32 [2048], P('tp'), may hold values from 0.1 to 1.9
- self_key_weight: float32 [2048], P('tp'), may hold values from -2 to 2
- mixer_output_weight: bfloat16 [2048, 2048], P('tp'), may hold values from -0.125 to 0.125
- second_batch_rows: bfloat16 [4096, 2048], P('ep'), may hold values from -6 to 6
- routed_expert_index: int32 [4096, 4], P('ep'), may hold values from 0 to 31, all different within a row; in each aligned block of 128 rows (0 to 127, 128 to 255, ...) at most 24 rows name the same one
- routing_output_weight: float32 [4096, 4], P('ep'), may hold values from 0.1 to 1
- expert_norm_gain: float32 [2048], replicated, may hold values from 0.1 to 1.9
- expert_gate_weight: bfloat16 [32, 1024, 2048], P('ep', 'tp'), may hold values from -0.125 to 0.125
- expert_up_weight: bfloat16 [32, 1024, 2048], P('ep', 'tp'), may hold values from -0.125 to 0.125
- expert_down_weight: bfloat16 [32, 1024, 2048], P('ep', None, 'tp'), may hold values from -0.1875 to 0.1875
- common_expert_gate: bfloat16 [1024, 2048], P('tp'), may hold values from -0.125 to 0.125
- common_expert_up: bfloat16 [1024, 2048], P('tp'), may hold values from -0.125 to 0.125
- common_expert_down: bfloat16 [1024, 2048], P(None, 'tp'), may hold values from -0.1875 to 0.1875
Outputs:
- token_mixer_output: bfloat16 [8192, 2048], P(('ep', 'tp'))
- expert_out: bfloat16 [4096, 2048], P('ep', 'tp')
Inputs may be any that keep to these rules, and one draw needn't show every extreme that they name: `routed_expert_index`: each row names 4 different experts. Within the rows of one index of ep no expert is named by more than 24 rows, and that bound is met in some index's rows.
All inputs are finite; a program needn't handle non-finite values.
Results may differ from a plain program's by a relative error of at most 0.017.
Values may be sent and summed in bfloat16 or wider, within the bound.
A program may use at most 64 MiB of HBM per device.

v0:
```python
import jax
import jax.numpy as jnp
from jax import lax
from jax.sharding import Mesh
from jax.sharding import PartitionSpec as P

HEAD_CHANNELS = 64
SPAN = 16
EP = ("ep_0", "ep_1")
EP_TP = ("ep_0", "ep_1", "tp")


HIGHEST = lax.Precision.HIGHEST
NORM_FLOOR = 1.0


def nothing_yet(array, identity):
    return jax.tree.map(
        lambda part, zero: jnp.zeros_like(part) + jnp.asarray(zero, part.dtype), array, identity
    )


def collected_together(array, axis):
    leaves = jax.tree.leaves(array)
    order = sorted(range(len(leaves)), key=lambda k: -leaves[k].size)
    width = (1, *leaves[order[0]].shape)[-1]
    lines = [
        jnp.pad(leaves[k].reshape(-1), (0, -leaves[k].size % width)).reshape(-1, width)
        for k in order
    ]
    both, at, found = (lax.all_gather(jnp.concatenate(lines), axis), 0, {})
    for k, line in zip(order, lines):
        piece = both[:, at : at + len(line)].reshape(len(both), -1)
        found[k] = piece[:, : leaves[k].size].reshape(-1, *leaves[k].shape)
        at += len(line)
    numbers = iter(range(len(leaves)))
    return jax.tree.map(lambda _: found[next(numbers)], array)


def prefix_by_axis(array, axes, combine, identity):
    before = start = nothing_yet(array, identity)
    total = array
    for axis in reversed(axes):
        size, mine = (lax.axis_size(axis), lax.axis_index(axis))
        pieces = collected_together(
            jax.tree.map(lambda part, kind: part.astype(kind), total, (jnp.bfloat16, jnp.bfloat16)),
            axis,
        )
        inside, total = (start, start)
        for k in range(size):
            passed = k < mine
            total = combine(
                total, jax.tree.map(lambda part, own: part[k].astype(own.dtype), pieces, array)
            )
            inside = jax.tree.map(lambda new, old: jnp.where(passed, new, old), total, inside)
        before = combine(inside, before)
    return before


def in_blocks(array, dim, size):
    lengths = array.shape
    pieces = array.reshape(*lengths[:dim], size, lengths[dim] // size, *lengths[dim + 1 :])
    return jnp.moveaxis(pieces, dim, 0)


def sent_and_summed(array, axis, dim):
    pieces = in_blocks(array, dim, lax.axis_size(axis))
    arrived = lax.all_to_all(pieces, axis, split_axis=0, concat_axis=0, tiled=True)
    return arrived.astype(jnp.float32).sum(axis=0)


def in_one_piece(arrays, axis, dim, along):
    ends, at = ([], 0)
    for a in arrays[:-1]:
        at += a.shape[along]
        ends.append(at)
    both = jnp.concatenate(arrays, axis=along)
    return tuple(jnp.split(lax.all_gather(both, axis, axis=dim, tiled=True), ends, axis=along))


def decay_terms(decay_data_input, correction_rate_input, decay_channel_offset):
    pre_log = -jax.nn.softplus(-(decay_channel_offset + decay_data_input.astype(jnp.float32))) - 0.5
    return (jnp.exp(-jnp.exp(pre_log)), jax.nn.sigmoid(correction_rate_input.astype(jnp.float32)))


def head_view(matrix):
    return matrix.astype(jnp.float32).reshape(matrix.shape[0], -1, HEAD_CHANNELS)


def complete_head_outputs(
    state_readout,
    receptance_rows,
    key_row_block,
    value_row_block,
    head_norm_gain,
    self_key_weight,
    mixer_output_gate,
):
    mean_part = jnp.mean(state_readout, axis=-1, keepdims=True)
    spread = jnp.mean(jnp.square(state_readout - mean_part), axis=-1, keepdims=True)
    normalized_rows = (state_readout - mean_part) * lax.rsqrt(spread + NORM_FLOOR)
    sequence_length = state_readout.shape[0]
    normalized_rows = normalized_rows.reshape(sequence_length, -1) * head_norm_gain
    self_key_term = (
        jnp.sum(
            receptance_rows * key_row_block * self_key_weight.reshape(-1, HEAD_CHANNELS),
            axis=-1,
            keepdims=True,
        )
        * value_row_block
    )
    mixer_result = (
        normalized_rows + self_key_term.reshape(sequence_length, -1)
    ) * mixer_output_gate.astype(jnp.float32)
    return mixer_result.astype(jnp.bfloat16)


def compose(earlier, later):
    first_move, first_sum = earlier
    second_move, second_sum = later
    moved = jnp.einsum("...ij,...jk->...ik", first_move, second_move, precision=HIGHEST)
    summed = (
        jnp.einsum("...ij,...jk->...ik", first_sum, second_move, precision=HIGHEST) + second_sum
    )
    return (moved, summed)


def mixer_part(
    receptance,
    key_tensor,
    value_tensor,
    decay_data_input,
    correction_rate_input,
    mixer_output_gate,
    decay_channel_offset,
    head_norm_gain,
    self_key_weight,
    mixer_output_weight,
):
    row_count, width = receptance.shape
    head_count = width // HEAD_CHANNELS
    block_count = row_count // SPAN
    decays, rates = decay_terms(decay_data_input, correction_rate_input, decay_channel_offset)
    receptance_rows = head_view(receptance)
    key_row_block = head_view(key_tensor)
    value_row_block = head_view(value_tensor)
    unit_keys = key_row_block * lax.rsqrt(
        jnp.sum(key_row_block * key_row_block, axis=-1, keepdims=True) + 1.0
    )
    decays = decays.reshape(key_row_block.shape)
    rates = rates.reshape(key_row_block.shape)

    def by_step(matrix):
        return matrix.reshape(block_count, SPAN, head_count, HEAD_CHANNELS).transpose(1, 0, 2, 3)

    eye_block = jnp.broadcast_to(
        jnp.eye(HEAD_CHANNELS, dtype=jnp.float32),
        (block_count, head_count, HEAD_CHANNELS, HEAD_CHANNELS),
    )
    initial = jnp.concatenate([jnp.zeros_like(eye_block), eye_block], axis=3)

    def advance(memory, inputs):
        recept_now, decay_now, key_now, value_now, unit_now, rate_now = inputs
        projected = jnp.einsum("ghji,ghj->ghi", memory, unit_now, precision=HIGHEST)
        memory = (
            memory * decay_now[..., None]
            - (unit_now * rate_now)[..., None] * projected[:, :, None, :]
        )
        fresh = key_now[..., None] * value_now[:, :, None, :]
        memory = memory.at[:, :, :, :HEAD_CHANNELS].add(fresh)
        return (memory, jnp.einsum("ghji,ghj->ghi", memory, recept_now, precision=HIGHEST))

    stepped = tuple(
        (
            by_step(matrix)
            for matrix in (
                receptance_rows,
                decays,
                key_row_block,
                value_row_block,
                unit_keys,
                rates,
            )
        )
    )
    final, state_readout = lax.scan(advance, initial, stepped)
    block_sums = jnp.swapaxes(final[..., :HEAD_CHANNELS], -1, -2)
    block_moves = jnp.swapaxes(final[..., HEAD_CHANNELS:], -1, -2)
    prefix_moves, prefix_sums = lax.associative_scan(compose, (block_moves, block_sums), axis=0)
    identity_move = jnp.broadcast_to(
        jnp.eye(HEAD_CHANNELS, dtype=jnp.float32), (head_count, HEAD_CHANNELS, HEAD_CHANNELS)
    )
    zero_sum = jnp.zeros_like(identity_move)
    _, carried = prefix_by_axis(
        (prefix_moves[-1], prefix_sums[-1]), EP, compose, (identity_move, zero_sum)
    )
    before_moves = jnp.concatenate([identity_move[None], prefix_moves[:-1]], axis=0)
    before_sums = jnp.concatenate([zero_sum[None], prefix_sums[:-1]], axis=0)
    starting = jnp.einsum("hij,ghjk->ghik", carried, before_moves, precision=HIGHEST) + before_sums
    local_reads = state_readout[..., :HEAD_CHANNELS]
    moved_reads = state_readout[..., HEAD_CHANNELS:]
    merged_output = local_reads + jnp.einsum(
        "ghij,lghj->lghi", starting, moved_reads, precision=HIGHEST
    )
    merged_output = merged_output.transpose(1, 0, 2, 3).reshape(
        row_count, head_count, HEAD_CHANNELS
    )
    mixer_result = complete_head_outputs(
        merged_output,
        receptance_rows,
        key_row_block,
        value_row_block,
        head_norm_gain,
        self_key_weight,
        mixer_output_gate,
    )
    return sent_and_summed(
        jnp.dot(mixer_result, mixer_output_weight, preferred_element_type=jnp.float32).astype(
            jnp.bfloat16
        ),
        "tp",
        0,
    ).astype(jnp.bfloat16)


def activate(rows_in, gate_part, up_part):
    pre_gate = jnp.einsum("fd,rd->fr", gate_part, rows_in, preferred_element_type=jnp.float32)
    pre_up = jnp.einsum("fd,rd->fr", up_part, rows_in, preferred_element_type=jnp.float32)
    return (jax.nn.silu(pre_gate) * pre_up).astype(jnp.bfloat16)


def expert_part(
    second_batch_rows,
    routed_expert_index,
    routing_output_weight,
    expert_norm_gain,
    expert_gate_weight,
    expert_up_weight,
    expert_down_weight,
    common_expert_gate,
    common_expert_up,
    common_expert_down,
):
    row_count, width = second_batch_rows.shape
    top_count = routed_expert_index.shape[1]
    peer_count = lax.axis_size(EP)
    slot_count = 3 * row_count * top_count // (2 * peer_count)
    out_width = expert_down_weight.shape[2]
    widened = second_batch_rows.astype(jnp.float32)
    normalized_rows = (
        widened
        * lax.rsqrt(jnp.mean(widened * widened, axis=-1, keepdims=True) + NORM_FLOOR)
        * expert_norm_gain
    ).astype(jnp.bfloat16)
    flat_ids = routed_expert_index.reshape(-1)
    one_hot = (flat_ids[:, None] == jnp.arange(peer_count, dtype=jnp.int32)[None, :]).astype(
        jnp.int32
    )
    slot_rank = jnp.sum((jnp.cumsum(one_hot, axis=0) - 1) * one_hot, axis=1)
    target = flat_ids * slot_count + slot_rank
    owners = jnp.arange(row_count * top_count, dtype=jnp.int32) // top_count
    source_row = jnp.full((peer_count * slot_count,), row_count, jnp.int32).at[target].set(owners)
    padded = jnp.concatenate([normalized_rows, jnp.zeros((1, width), jnp.bfloat16)], axis=0)
    outgoing = jnp.take(padded, source_row, axis=0).reshape(peer_count, slot_count, width)
    shared_hidden = activate(normalized_rows, common_expert_gate, common_expert_up)
    arrived = lax.all_to_all(outgoing, EP, split_axis=0, concat_axis=0, tiled=True)
    routed_hidden = activate(arrived.reshape(-1, width), expert_gate_weight[0], expert_up_weight[0])
    pieces = in_one_piece((routed_hidden, shared_hidden), "tp", 0, 1)
    routed_rows = expert_down_weight[0]
    routed_sum = jnp.einsum("fr,fd->rd", pieces[0], routed_rows, preferred_element_type=jnp.float32)
    shared_out = jnp.einsum(
        "fr,fd->rd", pieces[1], common_expert_down, preferred_element_type=jnp.float32
    )
    returned = lax.all_to_all(
        routed_sum.astype(jnp.bfloat16).reshape(peer_count, slot_count, out_width),
        EP,
        split_axis=0,
        concat_axis=0,
        tiled=True,
    )
    picked = jnp.take(returned.reshape(-1, out_width), target, axis=0).reshape(
        row_count, top_count, out_width
    )
    merged_output = (
        jnp.sum(picked.astype(jnp.float32) * routing_output_weight[:, :, None], axis=1) + shared_out
    )
    return merged_output.astype(jnp.bfloat16)


def on_device(
    receptance,
    key_tensor,
    value_tensor,
    decay_data_input,
    correction_rate_input,
    mixer_output_gate,
    decay_channel_offset,
    head_norm_gain,
    self_key_weight,
    mixer_output_weight,
    second_batch_rows,
    routed_expert_index,
    routing_output_weight,
    expert_norm_gain,
    expert_gate_weight,
    expert_up_weight,
    expert_down_weight,
    common_expert_gate,
    common_expert_up,
    common_expert_down,
):
    token_mixer_output = mixer_part(
        receptance,
        key_tensor,
        value_tensor,
        decay_data_input,
        correction_rate_input,
        mixer_output_gate,
        decay_channel_offset,
        head_norm_gain,
        self_key_weight,
        mixer_output_weight,
    )
    expert_out = expert_part(
        second_batch_rows,
        routed_expert_index,
        routing_output_weight,
        expert_norm_gain,
        expert_gate_weight,
        expert_up_weight,
        expert_down_weight,
        common_expert_gate,
        common_expert_up,
        common_expert_down,
    )
    return (token_mixer_output, expert_out)


def solution(mesh):
    split = Mesh(mesh.devices.reshape(16, 2, mesh.shape["tp"]), ("ep_0", "ep_1", "tp"))
    in_specs = (
        P(EP, "tp"),
        P(EP, "tp"),
        P(EP, "tp"),
        P(EP, "tp"),
        P(EP, "tp"),
        P(EP, "tp"),
        P("tp"),
        P("tp"),
        P("tp"),
        P("tp", None),
        P(EP, None),
        P(EP, None),
        P(EP, None),
        P(),
        P(EP, "tp", None),
        P(EP, "tp", None),
        P(EP, None, "tp"),
        P("tp", None),
        P("tp", None),
        P(None, "tp"),
    )
    out_specs = (P(EP_TP, None), P(EP, "tp"))
    return jax.shard_map(
        on_device, mesh=split, in_specs=in_specs, out_specs=out_specs, check_vma=False
    )
```

profile of v0, /device:TPU:6, one launch (start us, length us, event | category | flops | bytes accessed | tf_op | source)
XLA Modules:
  0.0 444.0 jit_solution(15981281089602616515)
XLA Ops:
  15.8 4.3 gather_fusion
  20.1 3.9 broadcast_select_fusion
  24.0 15.7 %all-to-all-start.1 = ((bf16[32,24,2048]{2,1,0:T(8,128)(2,1)}), bf16[32,24,2048]{2,1,0:T(8,128)(2,1)}, u32[]{:S(2)}, u32[]{:S(2)}) async-start(bf16[32,24,2048]{2,1,0:T(8,128)(2,1)} %broadcast_select_fusion), calls=%async_computation.1 | async-start | bytes 6291456 | tf_op jit(solution)/shard_map/all_to_all | solution.py:266
  46.2 157.8 %while.15 = (s32[]{:T(128)}, f32[16,2,64,128]{3,2,1,0:T(8,128)S(1)}, f32[16,16,2,128]{3,0,2,1:T(8,128)}, f32[16,16,2,64]{3,2,0,1:T(2,128)}, f32[16,16,2,64]{3,2,...) while((s32[]{:T(128)}, ...), condition=%wide.region_2.3_spmd, body=%wide.region_1.2_spmd.sunk | while | flops 7342082 | bytes 6529165 | solution.py:186
  206.0 2.8 slice_bitcast_fusion.1
  214.1 3.5 pad.58
  218.6 3.3 pad.60
  223.0 3.3 pad.59
  227.6 5.9 %pad.152 = f32[15,2,64,64]{3,2,1,0:T(8,128)} pad(f32[8,2,64,64]{3,2,1,0:T(8,128)S(1)} %add.279, f32[]{:T(128)} %constant.149.clone.1), padding=0_0_1x0_0_0x0_0_0x0_0_0 | pad | bytes 753668
  233.5 5.9 %pad.62 = f32[16,2,64,64]{3,2,1,0:T(8,128)} pad(f32[8,2,64,64]{3,2,1,0:T(8,128)S(1)} %add.279, f32[]{:T(128)} %constant.149.clone.1), padding=1_0_1x0_0_0x0_0_0x0_0_0 | pad | bytes 786436 | tf_op jit(solution)/shard_map/pad | solution.py:189
  250.8 3.3 pad.68
  255.4 3.3 pad.67
  260.0 6.0 %pad.70 = f32[16,2,64,64]{3,2,1,0:T(8,128)} pad(f32[8,2,64,64]{3,2,1,0:T(8,128)S(1)} %add.289, f32[]{:T(128)} %constant.149.clone.1), padding=1_0_1x0_0_0x0_0_0x0_0_0 | pad | bytes 786436 | tf_op jit(solution)/shard_map/pad | solution.py:189
  267.6 5.9 %pad.69 = f32[16,2,64,64]{3,2,1,0:T(8,128)} pad(f32[8,2,64,64]{3,2,1,0:T(8,128)S(1)} %pad_maximum_fusion.1, f32[]{:T(128)} %constant.149.clone.1), padding=0_1_1x0_0_0x0_0_0x0_0_0 | pad | bytes 786436 | tf_op jit(solution)/shard_map/pad | solution.py:189
  273.6 5.9 %pad.97 = f32[15,2,64,64]{3,2,1,0:T(8,128)} pad(f32[8,2,64,64]{3,2,1,0:T(8,128)S(1)} %pad_maximum_fusion.1, f32[]{:T(128)} %constant.149.clone.1), padding=0_0_1x0_0_0x0_0_0x0_0_0 | pad | bytes 753668 | tf_op jit(solution)/shard_map/slice | solution.py:198
  280.1 6.0 %pad.61 = f32[16,2,64,64]{3,2,1,0:T(8,128)} pad(f32[8,2,64,64]{3,2,1,0:T(8,128)S(1)} %pad_maximum_fusion, f32[]{:T(128)} %constant.149.clone.1), padding=0_1_1x0_0_0x0_0_0x0_0_0 | pad | bytes 786436 | tf_op jit(solution)/shard_map/pad | solution.py:189
  291.3 35.8 %all-gather.1 = bf16[4096,64]{1,0:T(8,128)(2,1)S(1)} all-gather(bf16[256,64]{1,0:T(8,128)(2,1)S(1)} %pad_maximum_fusion.8), channel_id=3, replica_groups=mesh['ep_0'=16,'ep_1'=2,'tp'=16] {'ep_0'}, dimensions={0}, use_global_device_ids=true | all-gather | bytes 557056 | tf_op jit(solution)/shard_map/all_gather | solution.py:31
  331.4 3.0 convolution_bitcast_fusion.4
  334.4 3.1 fusion.10
  346.1 7.5 %all-to-all-start = ((bf16[16,16,2048]{2,1,0:T(8,128)(2,1)}), bf16[16,16,2048]{2,1,0:T(8,128)(2,1)S(1)}, u32[]{:S(2)}, u32[]{:S(2)}) async-start(bf16[16,16,2048]{2,1,0:T(8,128)(2,1)} %bitcast.85), calls=%async_computation | async-start | bytes 2097152 | tf_op jit(solution)/shard_map/all_to_all | solution.py:68
  353.7 44.6 %all-gather.4.cloned.1.call-done = bf16[1024,896]{1,0:T(8,128)(2,1)} async-done(((bf16[64,896]{1,0:T(8,128)(2,1)}), bf16[1024,896]{1,0:T(8,128)(2,1)}) %all-gather.4.cloned.1.call-update) | async-done | bytes 1835024 | tf_op jit(solution)/shard_map/all_gather | solution.py:78
  398.3 2.7 fusion.4
  401.0 12.6 %all-to-all-start.2 = ((bf16[32,24,128]{2,1,0:T(8,128)(2,1)}), bf16[32,24,128]{2,1,0:T(8,128)(2,1)S(1)}, u32[]{:S(2)}, u32[]{:S(2)}) async-start(bf16[32,24,128]{2,1,0:T(8,128)(2,1)} %bitcast.98), calls=%async_computation.2 | async-start | bytes 393216 | tf_op jit(solution)/shard_map/all_to_all | solution.py:274
  414.8 18.7 %all-to-all-done.2 = bf16[32,24,128]{2,1,0:T(8,128)(2,1)S(1)} async-done(((bf16[32,24,128]{2,1,0:T(8,128)(2,1)}), bf16[32,24,128]{2,1,0:T(8,128)(2,1)S(1)}, u32[]{:S(2)}, u32[]{:S(2)}) %all-to-all-start.2) | async-done | bytes 196640 | tf_op jit(solution)/shard_map/all_to_all | solution.py:274
  (383 shorter events, 221.4 us)
Async XLA Ops:
  7.2 337.5 %copy-start = (bf16[128,2048]{1,0:T(8,128)(2,1)S(1)}, bf16[128,2048]{1,0:T(8,128)(2,1)}, u32[]{:S(2)}) copy-start(bf16[128,2048]{1,0:T(8,128)(2,1)} %param.33) | copy-start | bytes 1572868
  24.0 16.0 %copy-start.26 = (bf16[256,128]{1,0:T(8,128)(2,1)S(1)}, bf16[256,128]{1,0:T(8,128)(2,1)}, u32[]{:S(2)}) copy-start(bf16[256,128]{1,0:T(8,128)(2,1)} %param.25) | copy-start | bytes 196612
  24.0 16.3 %copy-start.27 = (bf16[256,128]{1,0:T(8,128)(2,1)S(1)}, bf16[256,128]{1,0:T(8,128)(2,1)}, u32[]{:S(2)}) copy-start(bf16[256,128]{1,0:T(8,128)(2,1)} %param.24) | copy-start | bytes 196612
  24.0 16.4 %copy-start.33 = (bf16[256,128]{1,0:T(8,128)(2,1)S(1)}, bf16[256,128]{1,0:T(8,128)(2,1)}, u32[]{:S(2)}) copy-start(bf16[256,128]{1,0:T(8,128)(2,1)} %param.27) | copy-start | bytes 196612
  24.0 16.4 %copy-start.34 = (f32[128]{0:T(128)S(1)}, f32[128]{0:T(128)}, u32[]{:S(2)}) copy-start(f32[128]{0:T(128)} %param.30) | copy-start | bytes 1540
  24.0 17.9 %copy-start.24 = (bf16[256,128]{1,0:T(8,128)(2,1)S(1)}, bf16[256,128]{1,0:T(8,128)(2,1)}, u32[]{:S(2)}) copy-start(bf16[256,128]{1,0:T(8,128)(2,1)} %param.28) | copy-start | bytes 196612
  24.0 18.8 %copy-start.17 = (bf16[256,128]{1,0:T(8,128)(2,1)S(1)}, bf16[256,128]{1,0:T(8,128)(2,1)}, u32[]{:S(2)}) copy-start(bf16[256,128]{1,0:T(8,128)(2,1)} %param.26) | copy-start | bytes 196612
  24.0 307.3 %all-to-all-start.1 = ((bf16[32,24,2048]{2,1,0:T(8,128)(2,1)}), bf16[32,24,2048]{2,1,0:T(8,128)(2,1)}, u32[]{:S(2)}, u32[]{:S(2)}) async-start(bf16[32,24,2048]{2,1,0:T(8,128)(2,1)} %broadcast_select_fusion), calls=%async_computation.1 | async-start | bytes 6291456 | tf_op jit(solution)/shard_map/all_to_all | solution.py:266
  39.8 358.5 %all-gather.4.cloned.1.call-start = ((), (), s32[]{:S(2)}) async-start(), calls=%async_computation.3 | async-start | bytes 1949696 | tf_op jit(solution)/shard_map/all_gather | solution.py:78
  40.1 4.6 %copy-start.7 = (bf16[256,128]{0,1:T(8,128)(2,1)}, bf16[256,128]{0,1:T(8,128)(2,1)S(1)}, u32[]{:S(2)}) copy-start(bf16[256,128]{0,1:T(8,128)(2,1)S(1)} %copy.81) | copy-start | bytes 196612
  239.4 4.7 %copy-start.6 = (f32[2,2,64,64]{3,2,1,0:T(8,128)S(1)}, f32[2,2,64,64]{3,2,1,0:T(8,128)}, u32[]{:S(2)}) copy-start(f32[2,2,64,64]{3,2,1,0:T(8,128)} %copy-done.5) | copy-start | bytes 196612
  244.9 10.5 %slice-start = ((f32[8,2,64,64]{3,2,1,0:T(8,128)}), f32[1,2,64,64]{3,2,1,0:T(8,128)S(1)}, s32[]{:S(2)}) async-start(f32[8,2,64,64]{3,2,1,0:T(8,128)} %copy-done.4), calls=%async_computation.4 | async-start | bytes 131072 | tf_op jit(solution)/shard_map/slice | solution.py:189
  255.4 12.2 %copy-start.20 = (f32[1,2,64,64]{3,2,1,0:T(8,128)S(1)}, f32[1,2,64,64]{3,2,1,0:T(8,128)}, u32[]{:S(2)}) copy-start(f32[1,2,64,64]{3,2,1,0:T(8,128)} %slice.454) | copy-start | bytes 98308
  267.6 12.5 %copy-start.19 = (f32[1,2,64,64]{3,2,1,0:T(8,128)S(1)}, f32[1,2,64,64]{3,2,1,0:T(8,128)}, u32[]{:S(2)}) copy-start(f32[1,2,64,64]{3,2,1,0:T(8,128)} %slice.443) | copy-start | bytes 98308
  291.3 39.2 %copy-start.13 = (bf16[64,2048]{1,0:T(8,128)(2,1)S(1)}, bf16[64,2048]{1,0:T(8,128)(2,1)}, u32[]{:S(2)}) copy-start(bf16[64,2048]{1,0:T(8,128)(2,1)} %param.41) | copy-start | bytes 786436
  340.1 4.6 %copy-start.18 = (bf16[256,128]{1,0:T(8,128)(2,1)S(1)}, bf16[256,128]{1,0:T(8,128)(2,1)}, u32[]{:S(2)}) copy-start(bf16[256,128]{1,0:T(8,128)(2,1)} %param.26) | copy-start | bytes 196612
  340.1 4.6 %copy-start.25 = (bf16[256,128]{1,0:T(8,128)(2,1)S(1)}, bf16[256,128]{1,0:T(8,128)(2,1)}, u32[]{:S(2)}) copy-start(bf16[256,128]{1,0:T(8,128)(2,1)} %param.29) | copy-start | bytes 196612
  340.1 4.6 %copy-start.30 = (f32[128]{0:T(128)S(1)}, f32[128]{0:T(128)}, u32[]{:S(2)}) copy-start(f32[128]{0:T(128)} %param.31) | copy-start | bytes 1540
  343.7 54.6 %copy-start.32 = (bf16[1,1024,128]{2,1,0:T(8,128)(2,1)S(1)}, bf16[1,1024,128]{2,1,0:T(8,128)(2,1)}, u32[]{:S(2)}) copy-start(bf16[1,1024,128]{2,1,0:T(8,128)(2,1)} %param.40) | copy-start | bytes 786436
  346.1 67.5 %copy-start.29 = (f32[128,4]{0,1:T(4,128)S(1)}, f32[128,4]{0,1:T(4,128)}, u32[]{:S(2)}) copy-start(f32[128,4]{0,1:T(4,128)} %param.36) | copy-start | bytes 6148
  346.1 67.7 %copy-start.28 = (s32[128,4]{0,1:T(4,128)S(1)}, s32[128,4]{0,1:T(4,128)}, u32[]{:S(2)}) copy-start(s32[128,4]{0,1:T(4,128)} %param.35) | copy-start | bytes 6148
  346.1 54.8 %all-to-all-start = ((bf16[16,16,2048]{2,1,0:T(8,128)(2,1)}), bf16[16,16,2048]{2,1,0:T(8,128)(2,1)S(1)}, u32[]{:S(2)}, u32[]{:S(2)}) async-start(bf16[16,16,2048]{2,1,0:T(8,128)(2,1)} %bitcast.85), calls=%async_computation | async-start | bytes 2097152 | tf_op jit(solution)/shard_map/all_to_all | solution.py:68
  353.7 81.6 %copy-start.21 = (bf16[1024,128]{1,0:T(8,128)(2,1)S(1)}, bf16[1024,128]{1,0:T(8,128)(2,1)}, u32[]{:S(2)}) copy-start(bf16[1024,128]{1,0:T(8,128)(2,1)} %param.43) | copy-start | bytes 786436
  401.0 32.6 %all-to-all-start.2 = ((bf16[32,24,128]{2,1,0:T(8,128)(2,1)}), bf16[32,24,128]{2,1,0:T(8,128)(2,1)S(1)}, u32[]{:S(2)}, u32[]{:S(2)}) async-start(bf16[32,24,128]{2,1,0:T(8,128)(2,1)} %bitcast.98), calls=%async_computation.2 | async-start | bytes 393216 | tf_op jit(solution)/shard_map/all_to_all | solution.py:274
  (17 other events, 48.1 us)
Sparse Core Ops, SparseCore 0:
  338.2 60.0 all-gather.3
where the time goes:
time: 450 us; the launch traced here: 444 us
  local copies, waits for them, and re-layouts  175 us (39%)
  waiting for transfers between devices  63.3 us (14%)
  matrix products  60.5 us (13%)
  other arithmetic  55.5 us (12%)
  blocking collectives  37.9 us (8%)
  starting transfers between devices  36.1 us (8%)
  between operations  15.2 us (3%)
    pad x12, local copies, waits for them, and re-layouts, mixer_part(): lax.associative_scan(compose, (block_moves, block_sums), axis=0)  46 us
    all_gather x1, waiting for transfers between devices, in_one_piece(): lax.all_gather(both, axis, axis=dim, tiled=True)  44.6 us
    all_gather x2, blocking collectives, collected_together(): both, at, found = (lax.all_gather(jnp.concatenate(lines), axis), 0, {})  37.9 us
    scatter-add x16, local copies, waits for them, and re-layouts, advance(): memory = memory.at[:, :, :, :HEAD_CHANNELS].add(fresh)  32 us
    dynamic_update_slice x16, local copies, waits for them, and re-layouts, mixer_part(): final, state_readout = lax.scan(advance, initial, stepped)  26.1 us
    all_to_all x1, waiting for transfers between devices, expert_part(): lax.all_to_all(routed_sum.astype(jnp.bfloat16).reshape(peer_count, slot_c...  18.7 us
    dot_general x16, matrix products, advance(): jnp.einsum('ghji,ghj->ghi', memory, recept_now, precision=HIGHEST)  16.2 us
    all_to_all x1, starting transfers between devices, expert_part(): lax.all_to_all(outgoing, EP, split_axis=0, concat_axis=0, tiled=True)  15.7 us
  transfers between devices with their start and end apart: 4, of which 2 were waited for; matrix products, arithmetic and copies ran while one was open for 59% of the time, Pallas kernels for 0%

commit v1 on v0

v1 whole, which is shorter than its diff:
```python
import functools

import jax
import jax.numpy as jnp
from jax import lax
from jax.experimental import pallas as pl
from jax.experimental.pallas import tpu as pltpu
from jax.sharding import Mesh
from jax.sharding import PartitionSpec as P

F32 = jnp.float32
BF16 = jnp.bfloat16
HEAD = 64
CHUNK = 64
RING = 4
CAP = 24
EXPERTS = 32
SOURCES = 8
MESH = pl.DeviceIdType.MESH
EP = ("z", "c")
TP = ("y", "x")
NN = (((1,), (0,)), ((), ()))
NT = (((1,), (1,)), ((), ()))
TN = (((0,), (0,)), ((), ()))


def dot(a, b, dims=NN):
    return lax.dot_general(a, b, dims, preferred_element_type=F32)


def halves(a):
    high = a.astype(BF16)
    return high, (a - high.astype(F32)).astype(BF16)


def dot3(a, b, dims=NN):
    (ah, al), (bh, bl) = a, b
    return dot(ah, bh, dims) + (dot(ah, bl, dims) + dot(al, bh, dims))


def dot_exact_left(a, b):
    b1 = b.astype(BF16)
    rest = b - b1.astype(F32)
    b2 = rest.astype(BF16)
    b3 = (rest - b2.astype(F32)).astype(BF16)
    return dot(a, b1) + (dot(a, b2) + dot(a, b3))


def dot_exact_right(a, b):
    ah, al = halves(a)
    return dot(ah, b) + dot(al, b)


def iota(shape, dim):
    return lax.broadcasted_iota(jnp.int32, shape, dim)


def copy_to(src, dst, send_sem, recv_sem, device):
    return pltpu.make_async_remote_copy(
        src_ref=src,
        dst_ref=dst,
        send_sem=send_sem,
        recv_sem=recv_sem,
        device_id=device,
        device_id_type=MESH,
    )


def silu(v):
    return v / (1.0 + jnp.exp(-v))


def local_mixer(rec_ref, key_ref, val_ref, dec_ref, rate_ref, off_ref, xg, yf, poll):
    n = 2 * CHUNK
    rows = rec_ref.shape[0]
    chunks = rows // CHUNK
    lane_head = iota((1, 128), 1) >> 6
    m0 = (lane_head == 0).astype(F32)
    m1 = 1.0 - m0
    same_head = ((iota((128, 128), 0) >> 6) == (iota((128, 128), 1) >> 6)).astype(BF16)
    i, j = iota((n, n), 0), iota((n, n), 1)
    eye = (i == j).astype(F32)
    same = (i >> 6) == (j >> 6)
    below = (i > j) & same
    upto = (i >= j) & same
    ri, rj = iota((rows, rows), 0), iota((rows, rows), 1)
    tri = ((ri >= rj) & ((ri >> 6) == (rj >> 6))).astype(F32).astype(BF16)

    key = key_ref[...].astype(F32)
    logw = -0.6065306597126334 / (1.0 + jnp.exp(-(off_ref[...] + dec_ref[...].astype(F32))))
    cum = dot_exact_left(tri, logw)
    rate = 1.0 / (1.0 + jnp.exp(-rate_ref[...].astype(F32)))
    unit = key * lax.rsqrt(dot_exact_right(key * key, same_head) + 1.0)
    b = unit * rate
    up = jnp.exp(cum)
    down = jnp.exp(-cum)
    u_t = unit * jnp.exp(cum - logw)
    r_t = rec_ref[...].astype(F32) * up
    k_t = key * down
    b_t = b * down
    value = val_ref[...].astype(F32)

    def part(a, at):
        return a[at * CHUNK : (at + 1) * CHUNK]

    def both(a):
        return jnp.concatenate([a * m0, a * m1], axis=0)

    every = range(chunks)
    end = [jnp.exp(part(cum, at)[CHUNK - 1 :]) for at in every]
    v2 = [both(part(value, at)) for at in every]
    v2h = [a.astype(BF16) for a in v2]
    u2 = [both(part(u_t, at)) for at in every]
    r2 = [both(part(r_t, at)) for at in every]
    b2 = [both(part(b_t, at)) for at in every]
    k2 = [both(part(k_t, at)) for at in every]
    left = [halves(jnp.concatenate([u2[at], r2[at]], axis=0)) for at in every]
    right = [halves(jnp.concatenate([b2[at], k2[at]], axis=0)) for at in every]
    pairs = [dot3(left[at], right[at], NT) for at in every]
    lower = [jnp.where(below, pairs[at][:n, :n], 0.0) for at in every]
    m_uk = [halves(jnp.where(below, pairs[at][:n, n:], 0.0)) for at in every]
    a_b = [halves(jnp.where(upto, pairs[at][n:, :n], 0.0)) for at in every]
    a_k = [halves(jnp.where(upto, pairs[at][n:, n:], 0.0)) for at in every]
    poll(0)
    mv = [dot(m_uk[at][0], v2h[at]) + dot(m_uk[at][1], v2h[at]) for at in every]
    akv = [dot(a_k[at][0], v2h[at]) + dot(a_k[at][1], v2h[at]) for at in every]
    inverse = None
    for level in range(6):
        half = (
            ((i >> (level + 1)) == (j >> (level + 1)))
            & (((i >> level) & 1) == 1)
            & (((j >> level) & 1) == 0)
        )
        step = [jnp.where(half, lower[at], 0.0) for at in every]
        if inverse is None:
            inverse = [eye - step[at] for at in every]
        else:
            split = [halves(inverse[at]) for at in every]
            mid = [dot3(halves(step[at]), split[at]) for at in every]
            inverse = [
                inverse[at] - dot3(split[at], halves(mid[at])) for at in every
            ]
    poll(1)
    ez = [
        halves(dot3(halves(inverse[at]), halves(jnp.concatenate([u2[at], mv[at]], axis=1))))
        for at in every
    ]
    aez = [dot3(a_b[at], ez[at]) for at in every]
    b_end = [halves(b2[at] * end[at]) for at in every]
    k_end = [halves(k2[at] * end[at]) for at in every]
    bez = [dot3(b_end[at], ez[at], TN) for at in every]
    kv = [dot(k_end[at][0], v2h[at], TN) + dot(k_end[at][1], v2h[at], TN) for at in every]
    poll(2)
    total = None
    for at in every:
        xo = r2[at] - aez[at][:, :128]
        yo = akv[at] - aez[at][:, 128:]
        xo = xo[:CHUNK] + xo[CHUNK:]
        yo = yo[:CHUNK] + yo[CHUNK:]
        moves = eye * end[at] - bez[at][:, :128]
        sums = kv[at] - bez[at][:, 128:]
        if total is None:
            xg[pl.ds(at * CHUNK, CHUNK), :] = xo
            yf[pl.ds(at * CHUNK, CHUNK), :] = yo
            total = jnp.concatenate([moves, sums], axis=1)
        else:
            ahead = halves(total)
            read = dot3(halves(xo), ahead)
            xg[pl.ds(at * CHUNK, CHUNK), :] = read[:, :128]
            yf[pl.ds(at * CHUNK, CHUNK), :] = read[:, 128:] + yo
            moved = dot3(halves(moves), ahead)
            total = jnp.concatenate([moved[:, :128], moved[:, 128:] + sums], axis=1)
    return total[:, :128], total[:, 128:]


def kernel(
    rec_ref,
    key_ref,
    val_ref,
    dec_ref,
    rate_ref,
    gate_ref,
    off_ref,
    gain_ref,
    self_ref,
    wout_hbm,
    rows_ref,
    idx_ref,
    wgt_ref,
    egain_ref,
    eg_hbm,
    eu_hbm,
    ed_hbm,
    cg_hbm,
    cu_hbm,
    cd_hbm,
    out0,
    out1,
    wout,
    gu,
    wd,
    cgu,
    cd,
    xn,
    sbuf,
    rbuf,
    hid,
    obuf,
    retb,
    pbuf,
    rcv,
    shb,
    q_hi,
    q_lo,
    onehot,
    xg,
    yf,
    cmap,
    pmap,
    zmine,
    zmap,
    sts,
    keep,
    ld,
    dsp_s,
    dsp_r,
    ys,
    yr,
    ws,
    wr,
    hs,
    hr,
    ret_s,
    ret_r,
    mx_s,
    mx_r,
    sh_s,
    sh_r,
    zs,
    zr,
    ps,
    pr,
):
    z, c = lax.axis_index("z"), lax.axis_index("c")
    y, x = lax.axis_index("y"), lax.axis_index("x")
    nz = lax.axis_size("z")
    ep, tp = 2 * z + c, RING * y + x
    home = ep % RING
    own = home == x
    mine = jnp.where(own, 1, 0)

    def at(z_=None, c_=None, y_=None, x_=None):
        return {
            "z": z if z_ is None else z_,
            "c": c if c_ is None else c_,
            "y": y if y_ is None else y_,
            "x": x if x_ is None else x_,
        }

    def place(e, y_=None, x_=None):
        return at(e // 2, e % 2, y_, x_)

    loads = [
        pltpu.make_async_copy(eg_hbm.at[0], gu.at[x, pl.ds(0, 64)], ld.at[0]),
        pltpu.make_async_copy(eu_hbm.at[0], gu.at[x, pl.ds(64, 64)], ld.at[1]),
        pltpu.make_async_copy(ed_hbm.at[0], wd.at[x], ld.at[2]),
        pltpu.make_async_copy(cg_hbm, cgu.at[pl.ds(0, 64)], ld.at[3]),
        pltpu.make_async_copy(cu_hbm, cgu.at[pl.ds(64, 64)], ld.at[4]),
        pltpu.make_async_copy(cd_hbm, cd, ld.at[5]),
        pltpu.make_async_copy(wout_hbm, wout, ld.at[6]),
    ]
    for load in loads:
        load.start()

    barrier = pltpu.get_barrier_semaphore()

    def tell(device):
        pl.semaphore_signal(barrier, inc=1, device_id=device, device_id_type=MESH)

    def tell_plane(k, _):
        @pl.when(k != tp)
        def _():
            tell(at(y_=k // RING, x_=k % RING))

        return 0

    lax.fori_loop(0, 16, tell_plane, 0)
    tell(at(c_=1 - c))

    def tell_later(k, _):
        tell(at(z_=k))
        return 0

    lax.fori_loop(0, z, tell_later, 0)

    def tell_source(k, _):
        @pl.when(RING * k + x != ep)
        def _():
            tell(place(RING * k + x))

        return 0

    lax.fori_loop(0, SOURCES, tell_source, 0)

    def tell_expert(e, _):
        @pl.when(jnp.logical_not((e == ep) & own))
        def _():
            tell(place(e, x_=home))

        return 0

    lax.fori_loop(0, EXPERTS, tell_expert, 0)

    rows = rows_ref[...].astype(F32)
    scale = lax.rsqrt(jnp.mean(rows * rows, axis=-1, keepdims=True) + 1.0)
    xn[...] = (rows * scale * egain_ref[...]).astype(BF16)

    row_count = rows_ref.shape[0]
    slots = EXPERTS * CAP
    lane_e = iota((row_count, EXPERTS), 1)
    chosen = jnp.zeros((row_count, EXPERTS), F32)
    weight = jnp.zeros((row_count, EXPERTS), F32)
    for k in range(4):
        hit = idx_ref[:, k : k + 1] == lane_e
        chosen = jnp.where(hit, 1.0, chosen)
        weight = jnp.where(hit, wgt_ref[:, k : k + 1], weight)
    earlier = (iota((row_count, row_count), 0) > iota((row_count, row_count), 1))
    rank = dot(earlier.astype(F32).astype(BF16), chosen.astype(BF16))
    label = jnp.where(chosen > 0.0, rank, -1.0).astype(BF16)
    slot_e, slot_s = iota((EXPERTS, slots), 0), iota((EXPERTS, slots), 1)
    spread = ((slot_s >= slot_e * CAP) & (slot_s < slot_e * CAP + CAP)).astype(F32)
    within = jnp.sum(spread * (slot_s - slot_e * CAP).astype(F32), axis=0, keepdims=True)
    spread = spread.astype(BF16)
    placed = (dot(label, spread) == within).astype(F32)
    w_hi, w_lo = halves(weight)
    q_hi[...] = (placed * dot(w_hi, spread)).astype(BF16)
    q_lo[...] = (placed * dot(w_lo, spread)).astype(BF16)

    onehot[...] = placed.astype(BF16)

    @pl.when(own)
    def _():
        features = xn[:, pl.ds(pl.multiple_of(512 * y, 512), 512)]
        packed = dot(onehot[...], features, TN)
        sbuf[...] = packed.reshape(EXPERTS, CAP, 512).astype(BF16)
        rbuf[y, ep // RING] = sbuf[ep]

    pl.semaphore_wait(barrier, 15 + 1 + (nz - 1 - z) + 31 * mine + 32 - mine)

    def dispatch(e):
        return copy_to(
            sbuf.at[e], rbuf.at[y, ep // RING], dsp_s.at[e], dsp_r.at[ep // RING], place(e)
        )

    @pl.when(own)
    def _():
        def send(k, _):
            dispatch((ep + k) % EXPERTS).start()
            return 0

        lax.fori_loop(1, EXPERTS, send, 0)

    def ring(piece, first_half, send_sem, recv_sem, p, axis):
        me = y if axis == "y" else x
        right, left, across = (me + 1) % RING, (me + 3) % RING, (me + 2) % RING

        def move(slot, way, to):
            device = at(y_=to) if axis == "y" else at(x_=to)
            return copy_to(piece(slot), piece(slot), send_sem.at[way, p], recv_sem.at[way, p], device)

        def start():
            move(me, 0, right).start()
            move(me, 1, left).start()

        def relay():
            if first_half:
                move(left, 0, right).wait_recv()
                move(left, 2, right).start()
            else:
                move(right, 1, left).wait_recv()
                move(right, 2, left).start()

        def near():
            if first_half:
                move(right, 1, left).wait_recv()
            else:
                move(left, 0, right).wait_recv()

        def far():
            move(across, 2, right).wait_recv()

        def sent():
            for way in range(3):
                move(me, way, right).wait_send()

        return start, relay, near, far, sent

    weights = [
        ring(lambda s: gu.at[s, pl.ds(0, 64)], True, ws, wr, 0, "x"),
        ring(lambda s: gu.at[s, pl.ds(64, 64)], False, ws, wr, 1, "x"),
        ring(lambda s: wd.at[s, pl.ds(0, 512)], True, ws, wr, 2, "x"),
        ring(lambda s: wd.at[s, pl.ds(512, 512)], False, ws, wr, 3, "x"),
    ]
    row_ring = [
        ring(lambda s, k=k: rbuf.at[s, k], k < SOURCES // 2, ys, yr, k, "y")
        for k in range(SOURCES)
    ]
    hid_ring = [
        ring(lambda s: hid.at[s, pl.ds(0, 96)], True, hs, hr, 0, "y"),
        ring(lambda s: hid.at[s, pl.ds(96, 96)], False, hs, hr, 1, "y"),
    ]
    for load in loads[:3]:
        load.wait()
    weights[0][0]()
    weights[1][0]()

    for load in loads[3:]:
        load.wait()
    pre = dot(cgu[...], xn[...], NT)
    shb[tp] = (silu(pre[:64]) * pre[64:]).astype(BF16)

    def share(k):
        return copy_to(
            shb.at[tp], shb.at[tp], sh_s.at[k], sh_r.at[tp], at(y_=k // RING, x_=k % RING)
        )

    def share_send(k, _):
        share((tp + k) % 16).start()
        return 0

    lax.fori_loop(1, 16, share_send, 0)

    def forward_rows():
        for k in range(SOURCES):
            @pl.when(RING * k + x != ep)
            def _():
                copy_to(
                    rbuf.at[y, k], rbuf.at[y, k], dsp_s.at[0], dsp_r.at[k], place(RING * k + x)
                ).wait_recv()

            row_ring[k][0]()

    def poll(stage):
        if stage == 0:
            pass
        elif stage == 1:
            weights[0][1]()
            weights[1][1]()
            weights[2][0]()
            weights[3][0]()
        else:
            forward_rows()

    moves, sums = local_mixer(
        rec_ref, key_ref, val_ref, dec_ref, rate_ref, off_ref, xg, yf, poll
    )
    cmap[0] = moves[:64] + pltpu.roll(sums[:64], 64, 1)
    cmap[1] = pltpu.roll(moves[64:], 64, 1) + sums[64:]

    swap = copy_to(cmap.at[1 - c], pmap, ps.at[0], pr.at[0], at(c_=1 - c))
    swap.start()
    for ring_of in row_ring:
        ring_of[1]()
    swap.wait_recv()
    lane = iota((64, 128), 1)
    first = jnp.where(c == 0, cmap[0], pmap[...])
    second = jnp.where(c == 0, pmap[...], cmap[1])

    def compose(later, earlier):
        stacked = jnp.concatenate([earlier, jnp.zeros_like(earlier)], axis=0)
        moved = dot3(halves(jnp.where(lane < 64, later, 0.0)), halves(stacked))
        return moved + jnp.where(lane < 64, 0.0, later)

    zmine[...] = compose(second, first).astype(BF16)

    def to_later(k):
        return copy_to(zmine, zmap.at[z], zs.at[k], zr.at[z], at(z_=k))

    def send_later(k, _):
        to_later(k).start()
        return 0

    lax.fori_loop(z + 1, nz, send_later, 0)

    weights[0][2]()
    weights[1][2]()
    weights[0][3]()
    weights[1][3]()

    def product(slot):
        taken = rbuf[slot].astype(F32).reshape(SOURCES * CAP, 512).astype(BF16)
        span = pl.ds(pl.multiple_of(512 * slot, 512), 512)
        g = gu[:, 0:64, span].reshape(256, 512)
        u = gu[:, 64:128, span].reshape(256, 512)
        return dot(taken, g, NT), dot(taken, u, NT)

    g0, u0 = product(y)
    for ring_of in row_ring:
        ring_of[2]()
    g1, u1 = product((y + 1) % RING)
    g2, u2 = product((y + 3) % RING)
    for ring_of in row_ring:
        ring_of[3]()
    g3, u3 = product((y + 2) % RING)
    hidden = silu((g0 + g1) + (g2 + g3)) * ((u0 + u1) + (u2 + u3))
    hid[y] = hidden.astype(BF16)
    hid_ring[0][0]()
    hid_ring[1][0]()
    weights[2][1]()
    weights[3][1]()

    keep[...] = jnp.zeros((64, 128), F32)

    def advance(k, _):
        copy_to(zmine, zmap.at[k], zs.at[0], zr.at[k], at(z_=k)).wait_recv()
        step = zmap[k].astype(F32)
        low = jnp.where(lane < 64, step, 0.0)
        twice = (low + pltpu.roll(low, 64, 1)).astype(BF16)
        s_hi, s_lo = halves(keep[...])
        moved = dot(twice, jnp.concatenate([s_hi, s_lo], axis=0))
        keep[...] = moved + jnp.where(lane < 64, 0.0, step)
        return 0

    lax.fori_loop(0, z, advance, 0)
    state = keep[...]
    passed = jnp.where(lane < 64, 0.0, compose(first, state))
    sts[c] = jnp.where(c == 0, state, passed)
    keep[...] = jnp.where(c == 0, passed, state)
    hand = copy_to(keep, sts.at[c], ps.at[1], pr.at[1], at(c_=1 - c))
    hand.start()
    hid_ring[0][1]()
    hid_ring[1][1]()
    copy_to(keep, sts.at[1 - c], ps.at[1], pr.at[1], at(c_=1 - c)).wait_recv()

    start = jnp.concatenate([pltpu.roll(sts[0], 64, 1), sts[1]], axis=0)
    readout = dot3(halves(xg[...]), halves(start)) + yf[...]
    same_head = ((iota((128, 128), 0) >> 6) == (iota((128, 128), 1) >> 6)).astype(F32)
    mean_of = (same_head * (1.0 / HEAD)).astype(BF16)
    same_head = same_head.astype(BF16)
    centred = readout - dot_exact_right(readout, mean_of)
    variance = dot_exact_right(centred * centred, mean_of)
    key = key_ref[...].astype(F32)
    bonus = dot_exact_right(rec_ref[...].astype(F32) * key * self_ref[...], same_head)
    mixed = (
        centred * lax.rsqrt(variance + 1.0) * gain_ref[...] + bonus * val_ref[...].astype(F32)
    ) * gate_ref[...].astype(F32)
    mixed = mixed.astype(BF16)

    def give(k):
        return copy_to(
            pbuf.at[k], rcv.at[tp], mx_s.at[k], mx_r.at[tp], at(y_=k // RING, x_=k % RING)
        )

    for group in range(4):
        partial = dot(mixed[64 * group : 64 * group + 64], wout[...])
        pbuf[4 * group : 4 * group + 4] = partial.reshape(4, 16, 2048).astype(BF16)
        for k in range(4 * group, 4 * group + 4):
            @pl.when(k != tp)
            def _():
                give(k).start()

    rcv[tp] = pbuf[tp]

    weights[2][2]()
    weights[3][2]()
    weights[2][3]()
    weights[3][3]()
    for ring_of in hid_ring:
        ring_of[2]()
        ring_of[3]()
    for s in range(RING):
        made = dot(hid[0], wd[s, 0:256])
        for part in range(1, RING):
            made = made + dot(hid[part], wd[s, 256 * part : 256 * part + 256])
        obuf[s] = made.reshape(SOURCES, CAP, 128).astype(BF16)

    def give_back(k, s):
        return copy_to(
            obuf.at[s, k],
            retb.at[ep],
            ret_s.at[RING * k + s],
            ret_r.at[ep],
            place(RING * k + x, x_=s),
        )

    def send_back(n, _):
        k, s = n // RING, n % RING
        @pl.when(jnp.logical_not((RING * k + x == ep) & (s == x)))
        def _():
            give_back(k, s).start()

        return 0

    lax.fori_loop(0, EXPERTS, send_back, 0)

    @pl.when(own)
    def _():
        retb[ep] = obuf[x, ep // RING]

    def take(k, _):
        copy_to(
            pbuf.at[0], rcv.at[k], mx_s.at[0], mx_r.at[k], at(y_=k // RING, x_=k % RING)
        ).wait_recv()
        return 0

    def take_other(k, _):
        @pl.when(k != tp)
        def _():
            take(k, 0)

        return 0

    lax.fori_loop(0, 16, take_other, 0)
    summed = rcv[0].astype(F32)
    for k in range(1, 16):
        summed = summed + rcv[k].astype(F32)
    out0[...] = summed.astype(BF16)

    def shared_in(k, _):
        @pl.when(k != tp)
        def _():
            copy_to(
                shb.at[k], shb.at[k], sh_s.at[0], sh_r.at[k], at(y_=k // RING, x_=k % RING)
            ).wait_recv()

        return 0

    lax.fori_loop(0, 16, shared_in, 0)
    shared = dot(shb[...].reshape(1024, 128), cd[...], TN)

    def back_in(e, _):
        @pl.when(jnp.logical_not((e == ep) & own))
        def _():
            copy_to(
                retb.at[e], retb.at[e], ret_s.at[0], ret_r.at[e], place(e, x_=home)
            ).wait_recv()

        return 0

    lax.fori_loop(0, EXPERTS, back_in, 0)
    copies = retb[...].astype(F32).reshape(slots, 128).astype(BF16)
    merged = dot(q_hi[...], copies) + dot(q_lo[...], copies) + shared
    out1[...] = merged.astype(BF16)

    @pl.when(own)
    def _():
        def sent(k, _):
            dispatch((ep + k) % EXPERTS).wait_send()
            return 0

        lax.fori_loop(1, EXPERTS, sent, 0)

    for ring_of in weights + row_ring + hid_ring:
        ring_of[4]()
    swap.wait_send()
    hand.wait_send()

    def later_sent(k, _):
        to_later(k).wait_send()
        return 0

    lax.fori_loop(z + 1, nz, later_sent, 0)

    def plane_sent(k, _):
        @pl.when(k != tp)
        def _():
            give(k).wait_send()
            share(k).wait_send()

        return 0

    lax.fori_loop(0, 16, plane_sent, 0)

    def back_sent(n, _):
        k, s = n // RING, n % RING
        @pl.when(jnp.logical_not((RING * k + x == ep) & (s == x)))
        def _():
            give_back(k, s).wait_send()

        return 0

    lax.fori_loop(0, EXPERTS, back_sent, 0)


def on_device(
    receptance,
    key_tensor,
    value_tensor,
    decay_data_input,
    correction_rate_input,
    mixer_output_gate,
    decay_channel_offset,
    head_norm_gain,
    self_key_weight,
    mixer_output_weight,
    second_batch_rows,
    routed_expert_index,
    routing_output_weight,
    expert_norm_gain,
    expert_gate_weight,
    expert_up_weight,
    expert_down_weight,
    common_expert_gate,
    common_expert_up,
    common_expert_down,
):
    vmem = pl.BlockSpec(memory_space=pltpu.VMEM)
    hbm = pl.BlockSpec(memory_space=pl.ANY)
    dma = pltpu.SemaphoreType.DMA
    scratch = [
        pltpu.VMEM((128, 2048), BF16),
        pltpu.VMEM((RING, 128, 2048), BF16),
        pltpu.VMEM((RING, 1024, 128), BF16),
        pltpu.VMEM((128, 2048), BF16),
        pltpu.VMEM((1024, 128), BF16),
        pltpu.VMEM((128, 2048), BF16),
        pltpu.VMEM((EXPERTS, CAP, 512), BF16),
        pltpu.VMEM((RING, SOURCES, CAP, 512), BF16),
        pltpu.VMEM((RING, SOURCES * CAP, 256), BF16),
        pltpu.VMEM((RING, SOURCES, CAP, 128), BF16),
        pltpu.VMEM((EXPERTS, CAP, 128), BF16),
        pltpu.VMEM((16, 16, 2048), BF16),
        pltpu.VMEM((16, 16, 2048), BF16),
        pltpu.VMEM((16, 64, 128), BF16),
        pltpu.VMEM((128, EXPERTS * CAP), BF16),
        pltpu.VMEM((128, EXPERTS * CAP), BF16),
        pltpu.VMEM((128, EXPERTS * CAP), BF16),
        pltpu.VMEM((256, 128), F32),
        pltpu.VMEM((256, 128), F32),
        pltpu.VMEM((2, 64, 128), F32),
        pltpu.VMEM((64, 128), F32),
        pltpu.VMEM((64, 128), BF16),
        pltpu.VMEM((16, 64, 128), BF16),
        pltpu.VMEM((2, 64, 128), F32),
        pltpu.VMEM((64, 128), F32),
        dma((8,)),
        dma((EXPERTS,)),
        dma((SOURCES,)),
        dma((3, SOURCES)),
        dma((3, SOURCES)),
        dma((3, 4)),
        dma((3, 4)),
        dma((3, 2)),
        dma((3, 2)),
        dma((EXPERTS,)),
        dma((EXPERTS,)),
        dma((16,)),
        dma((16,)),
        dma((16,)),
        dma((16,)),
        dma((16,)),
        dma((16,)),
        dma((2,)),
        dma((2,)),
    ]
    return pl.pallas_call(
        kernel,
        out_shape=(
            jax.ShapeDtypeStruct((16, 2048), BF16),
            jax.ShapeDtypeStruct((128, 128), BF16),
        ),
        in_specs=[vmem] * 9 + [hbm] + [vmem] * 4 + [hbm] * 6,
        out_specs=(vmem, vmem),
        scratch_shapes=scratch,
        compiler_params=pltpu.CompilerParams(
            collective_id=0, has_side_effects=True, vmem_limit_bytes=60 * 1024 * 1024
        ),
        name="mixer_and_experts",
    )(
        receptance,
        key_tensor,
        value_tensor,
        decay_data_input,
        correction_rate_input,
        mixer_output_gate,
        decay_channel_offset.reshape(1, 128),
        head_norm_gain.reshape(1, 128),
        self_key_weight.reshape(1, 128),
        mixer_output_weight,
        second_batch_rows,
        routed_expert_index,
        routing_output_weight,
        expert_norm_gain.reshape(1, 2048),
        expert_gate_weight,
        expert_up_weight,
        expert_down_weight,
        common_expert_gate,
        common_expert_up,
        common_expert_down,
    )


def solution(mesh):
    split = Mesh(mesh.devices.reshape(16, 2, 4, 4), ("z", "c", "y", "x"))
    in_specs = (
        P(EP, TP),
        P(EP, TP),
        P(EP, TP),
        P(EP, TP),
        P(EP, TP),
        P(EP, TP),
        P(TP),
        P(TP),
        P(TP),
        P(TP, None),
        P(EP, None),
        P(EP, None),
        P(EP, None),
        P(),
        P(EP, TP, None),
        P(EP, TP, None),
        P(EP, None, TP),
        P(TP, None),
        P(TP, None),
        P(None, TP),
    )
    out_specs = (P(EP + TP, None), P(EP, TP))
    return jax.shard_map(
        on_device, mesh=split, in_specs=in_specs, out_specs=out_specs, check_vma=False
    )
```

time: 450 us -> 87.4 us (0.19); the launches traced: 444 us -> 86.7 us
  local copies, waits for them, and re-layouts: 175 us -> 4.24 us
  Pallas kernels: 0 us -> 81.8 us
  waiting for transfers between devices: 63.3 us -> 0 us
  matrix products: 60.5 us -> 0 us
  other arithmetic: 55.5 us -> 0 us
  blocking collectives: 37.9 us -> 0 us
  starting transfers between devices: 36.1 us -> 0 us
  between operations: 15.2 us -> 0.66 us
    pallas_call x0 -> x1, Pallas kernels: none -> 81.8 us  [on_device(): pl.pallas_call(kernel, out_shape=(jax.ShapeDtypeStruct((16, 2048), BF16),...]
    dot_general x78 -> x0, matrix products: 60.5 us -> none  [the longest x16 16.2 us: advance(): jnp.einsum('ghji,ghj->ghi', memory, recept_now, precision=HIGHEST)]
    pad x12 -> x0, local copies, waits for them, and re-layouts: 46 us -> none  [mixer_part(): lax.associative_scan(compose, (block_moves, block_sums), axis=0)]
    all_gather x1 -> x0, waiting for transfers between devices: 44.6 us -> none  [in_one_piece(): lax.all_gather(both, axis, axis=dim, tiled=True)]
    all_gather x2 -> x0, blocking collectives: 37.9 us -> none  [collected_together(): both, at, found = (lax.all_gather(jnp.concatenate(lines), axis), 0, {})]
    all_to_all x3 -> x0, starting transfers between devices: 35.9 us -> none  [the longest x1 15.7 us: expert_part(): lax.all_to_all(outgoing, EP, split_axis=0, concat_axis=0, tiled=True)]
    scatter-add x16 -> x0, local copies, waits for them, and re-layouts: 32 us -> none  [advance(): memory = memory.at[:, :, :, :HEAD_CHANNELS].add(fresh)]
    dynamic_update_slice x16 -> x0, local copies, waits for them, and re-layouts: 26.1 us -> none  [mixer_part(): final, state_readout = lax.scan(advance, initial, stepped)]
  transfers between devices with their start and end apart: 4 -> 0, of which waited for: 2 -> 0; matrix products, arithmetic and copies ran while one was open for 59% -> 0% of each run, Pallas kernels for 0% -> 0%
where the time goes in v1:
time: 87.4 us; the launch traced here: 86.7 us
  Pallas kernels  81.8 us (94%)
  local copies, waits for them, and re-layouts  4.24 us (5%)
    pallas_call x1, Pallas kernels, on_device(): pl.pallas_call(kernel, out_shape=(jax.ShapeDtypeStruct((16, 2048), BF16),...  81.8 us
    unnamed x10, local copies, waits for them, and re-layouts  4.24 us

profile of v1, /device:TPU:6, one launch (start us, length us, event | category | flops | bytes accessed | tf_op | source)
XLA Modules:
  0.0 86.7 jit_solution(1255619365114900592)
XLA Ops:
  0.6 0.0 copy-start.1
  0.6 0.7 copy-done.1
  1.3 0.0 copy-start.2
  1.3 0.7 copy.22.idx_ref
  2.1 0.0 copy-done.2
  2.1 0.7 copy.23.wgt_ref
  2.8 81.8 %mixer_and_experts.1 = (bf16[16,2048]{1,0:T(8,128)(2,1)}, bf16[128,128]{1,0:T(8,128)(2,1)}) custom-call(bf16[256,128]{1,0:T(8,128)(2,1)} %rec_ref.1, bf16[256,128]{1,0:T(8,128)(2,1)} %key_ref.1, bf16[256,128]{1,0:T(8,128)(2,1)} %val_ref.1, bf16[256,128]{1,0:T(8,128)(2,1)} %dec_ref.1, bf16[256,128]{1,0:T(8,128)(2,1)} %rate_ref.1, bf16[256,128]{1,0:T(8,128)(2,1)} %gate_ref.1, ...), custom_call_target="tpu_custom_call" | custom-call | tf_op jit(solution)/shard_map/mixer_and_experts/pallas_call | solution.py:756
  84.6 0.0 copy-start
  84.6 1.5 %copy.26 = bf16[16,2048]{1,0:T(8,128)(2,1)} copy(bf16[16,2048]{1,0:T(8,128)(2,1)} %get-tuple-element.4) | data formatting | bytes 131072
  86.1 0.0 copy-done
  86.1 0.6 copy.27
Async XLA Ops:
  0.6 0.7 copy-start.1
  1.3 0.7 copy-start.2
  84.6 1.5 %copy-start = (bf16[128,128]{1,0:T(8,128)(2,1)S(1)}, bf16[128,128]{1,0:T(8,128)(2,1)}, u32[]{:S(2)}) copy-start(bf16[128,128]{1,0:T(8,128)(2,1)} %get-tuple-element.5) | copy-start | bytes 98308

commit v2 on v1

v2 whole, which is shorter than its diff:
```python
import functools

import jax
import jax.numpy as jnp
from jax import lax
from jax.experimental import pallas as pl
from jax.experimental.pallas import tpu as pltpu
from jax.sharding import Mesh
from jax.sharding import PartitionSpec as P

F32 = jnp.float32
BF16 = jnp.bfloat16
HEAD = 64
CHUNK = 64
RING = 4
CAP = 24
EXPERTS = 32
SOURCES = 8
MESH = pl.DeviceIdType.MESH
EP = ("z", "c")
TP = ("y", "x")
NN = (((1,), (0,)), ((), ()))
NT = (((1,), (1,)), ((), ()))
TN = (((0,), (0,)), ((), ()))


def dot(a, b, dims=NN):
    return lax.dot_general(a, b, dims, preferred_element_type=F32)


def halves(a):
    high = a.astype(BF16)
    return high, (a - high.astype(F32)).astype(BF16)


def dot3(a, b, dims=NN):
    (ah, al), (bh, bl) = a, b
    return dot(ah, bh, dims) + (dot(ah, bl, dims) + dot(al, bh, dims))


def dot_exact_left(a, b):
    b1 = b.astype(BF16)
    rest = b - b1.astype(F32)
    b2 = rest.astype(BF16)
    b3 = (rest - b2.astype(F32)).astype(BF16)
    return dot(a, b1) + (dot(a, b2) + dot(a, b3))


def dot_exact_right(a, b):
    ah, al = halves(a)
    return dot(ah, b) + dot(al, b)


def iota(shape, dim):
    return lax.broadcasted_iota(jnp.int32, shape, dim)


def copy_to(src, dst, send_sem, recv_sem, device):
    return pltpu.make_async_remote_copy(
        src_ref=src,
        dst_ref=dst,
        send_sem=send_sem,
        recv_sem=recv_sem,
        device_id=device,
        device_id_type=MESH,
    )


def silu(v):
    return v / (1.0 + jnp.exp(-v))


def local_mixer(rec_ref, key_ref, val_ref, dec_ref, rate_ref, off_ref, xg, yf):
    n = 2 * CHUNK
    rows = rec_ref.shape[0]
    chunks = rows // CHUNK
    lane_head = iota((1, 128), 1) >> 6
    m0 = (lane_head == 0).astype(F32)
    m1 = 1.0 - m0
    same_head = ((iota((128, 128), 0) >> 6) == (iota((128, 128), 1) >> 6)).astype(BF16)
    i, j = iota((n, n), 0), iota((n, n), 1)
    eye = (i == j).astype(F32)
    same = (i >> 6) == (j >> 6)
    below = (i > j) & same
    upto = (i >= j) & same
    ri, rj = iota((rows, rows), 0), iota((rows, rows), 1)
    tri = ((ri >= rj) & ((ri >> 6) == (rj >> 6))).astype(F32).astype(BF16)

    key = key_ref[...].astype(F32)
    logw = -0.6065306597126334 / (1.0 + jnp.exp(-(off_ref[...] + dec_ref[...].astype(F32))))
    cum = dot_exact_left(tri, logw)
    rate = 1.0 / (1.0 + jnp.exp(-rate_ref[...].astype(F32)))
    unit = key * lax.rsqrt(dot_exact_right(key * key, same_head) + 1.0)
    b = unit * rate
    up = jnp.exp(cum)
    down = jnp.exp(-cum)
    u_t = unit * jnp.exp(cum - logw)
    r_t = rec_ref[...].astype(F32) * up
    k_t = key * down
    b_t = b * down
    value = val_ref[...].astype(F32)

    def part(a, at):
        return a[at * CHUNK : (at + 1) * CHUNK]

    def both(a):
        return jnp.concatenate([a * m0, a * m1], axis=0)

    every = range(chunks)
    end = [jnp.exp(part(cum, at)[CHUNK - 1 :]) for at in every]
    v2 = [both(part(value, at)) for at in every]
    v2h = [a.astype(BF16) for a in v2]
    u2 = [both(part(u_t, at)) for at in every]
    r2 = [both(part(r_t, at)) for at in every]
    b2 = [both(part(b_t, at)) for at in every]
    k2 = [both(part(k_t, at)) for at in every]
    left = [halves(jnp.concatenate([u2[at], r2[at]], axis=0)) for at in every]
    right = [halves(jnp.concatenate([b2[at], k2[at]], axis=0)) for at in every]
    pairs = [dot3(left[at], right[at], NT) for at in every]
    lower = [jnp.where(below, pairs[at][:n, :n], 0.0) for at in every]
    m_uk = [halves(jnp.where(below, pairs[at][:n, n:], 0.0)) for at in every]
    a_b = [halves(jnp.where(upto, pairs[at][n:, :n], 0.0)) for at in every]
    a_k = [halves(jnp.where(upto, pairs[at][n:, n:], 0.0)) for at in every]
    mv = [dot(m_uk[at][0], v2h[at]) + dot(m_uk[at][1], v2h[at]) for at in every]
    akv = [dot(a_k[at][0], v2h[at]) + dot(a_k[at][1], v2h[at]) for at in every]
    inverse = None
    for level in range(6):
        half = (
            ((i >> (level + 1)) == (j >> (level + 1)))
            & (((i >> level) & 1) == 1)
            & (((j >> level) & 1) == 0)
        )
        step = [jnp.where(half, lower[at], 0.0) for at in every]
        if inverse is None:
            inverse = [eye - step[at] for at in every]
        else:
            split = [halves(inverse[at]) for at in every]
            mid = [dot3(halves(step[at]), split[at]) for at in every]
            inverse = [
                inverse[at] - dot3(split[at], halves(mid[at])) for at in every
            ]
    ez = [
        halves(dot3(halves(inverse[at]), halves(jnp.concatenate([u2[at], mv[at]], axis=1))))
        for at in every
    ]
    aez = [dot3(a_b[at], ez[at]) for at in every]
    b_end = [halves(b2[at] * end[at]) for at in every]
    k_end = [halves(k2[at] * end[at]) for at in every]
    bez = [dot3(b_end[at], ez[at], TN) for at in every]
    kv = [dot(k_end[at][0], v2h[at], TN) + dot(k_end[at][1], v2h[at], TN) for at in every]
    total = None
    for at in every:
        xo = r2[at] - aez[at][:, :128]
        yo = akv[at] - aez[at][:, 128:]
        xo = xo[:CHUNK] + xo[CHUNK:]
        yo = yo[:CHUNK] + yo[CHUNK:]
        moves = eye * end[at] - bez[at][:, :128]
        sums = kv[at] - bez[at][:, 128:]
        if total is None:
            xg[pl.ds(at * CHUNK, CHUNK), :] = xo
            yf[pl.ds(at * CHUNK, CHUNK), :] = yo
            total = jnp.concatenate([moves, sums], axis=1)
        else:
            ahead = halves(total)
            read = dot3(halves(xo), ahead)
            xg[pl.ds(at * CHUNK, CHUNK), :] = read[:, :128]
            yf[pl.ds(at * CHUNK, CHUNK), :] = read[:, 128:] + yo
            moved = dot3(halves(moves), ahead)
            total = jnp.concatenate([moved[:, :128], moved[:, 128:] + sums], axis=1)
    return total[:, :128], total[:, 128:]


def kernel(*refs):
    (
        rec_in,
        key_in,
        val_in,
        dec_in,
        rate_in,
        gate_in,
        off_in,
        gain_in,
        self_in,
        wout_in,
        rows_in,
        idx_in,
        wgt_in,
        egain_in,
        eg_in,
        eu_in,
        ed_in,
        cg_in,
        cu_in,
        cd_in,
        out0,
        out1,
    ) = refs[:22]
    (
        rec_ref,
        key_ref,
        val_ref,
        dec_ref,
        rate_ref,
        gate_ref,
        off_ref,
        gain_ref,
        self_ref,
        rows_ref,
        idx_ref,
        wgt_ref,
        egain_ref,
        wout,
        gu,
        wd,
        cgu,
        cd,
        xn,
        sbuf,
        rbuf,
        hid,
        obuf,
        retb,
        pb0,
        pb1,
        qb0,
        qb1,
        gh0,
        gh1,
        gh2,
        gh3,
        gp0,
        gp1,
        gp2,
        gp3,
        shb,
        q_hi,
        q_lo,
        onehot,
        xg,
        yf,
        cmap,
        pmap,
        zmine,
        zmap,
        zlast,
        zall,
        sts,
        keep,
        ahead,
        res0,
        res1,
    ) = refs[22:75]
    (
        ld,
        dsp_s,
        dsp_r,
        ys,
        yr,
        ws,
        wr,
        hs,
        hr,
        ret_s,
        ret_r,
        rs_s,
        rs_h,
        rs_p,
        sh_s,
        sh_r,
        zs,
        zr,
        zls,
        zlr,
        od,
        ps,
        pr,
    ) = refs[75:]
    z, c = lax.axis_index("z"), lax.axis_index("c")
    y, x = lax.axis_index("y"), lax.axis_index("x")
    nz = lax.axis_size("z")
    ep, tp = 2 * z + c, RING * y + x
    home = ep % RING
    own = home == x
    mine = jnp.where(own, 1, 0)
    group, inner = z // RING, z % RING
    last = inner == RING - 1
    later = nz - RING * (group + 1)

    def at(z_=None, c_=None, y_=None, x_=None):
        return {
            "z": z if z_ is None else z_,
            "c": c if c_ is None else c_,
            "y": y if y_ is None else y_,
            "x": x if x_ is None else x_,
        }

    def place(e, y_=None, x_=None):
        return at(e // 2, e % 2, y_, x_)

    loads = []
    for source, target in (
        (rows_in, rows_ref),
        (egain_in, egain_ref),
        (idx_in, idx_ref),
        (wgt_in, wgt_ref),
        (key_in, key_ref),
        (dec_in, dec_ref),
        (off_in, off_ref),
        (rate_in, rate_ref),
        (rec_in, rec_ref),
        (val_in, val_ref),
        (eg_in.at[0], gu.at[x, pl.ds(0, 64)]),
        (eu_in.at[0], gu.at[x, pl.ds(64, 64)]),
        (cg_in, cgu.at[pl.ds(0, 64)]),
        (cu_in, cgu.at[pl.ds(64, 64)]),
        (ed_in.at[0], wd.at[x]),
        (cd_in, cd),
        (wout_in, wout),
        (gate_in, gate_ref),
        (gain_in, gain_ref),
        (self_in, self_ref),
    ):
        loads.append(pltpu.make_async_copy(source, target, ld.at[len(loads)]))
        loads[-1].start()

    barrier = pltpu.get_barrier_semaphore()

    def tell(device):
        pl.semaphore_signal(barrier, inc=1, device_id=device, device_id_type=MESH)

    def tell_source(k, _):
        source = RING * ((ep // RING + 4 + k) % SOURCES) + x

        @pl.when(source != ep)
        def _():
            tell(place(source))

        return 0

    lax.fori_loop(0, SOURCES, tell_source, 0)

    def tell_expert(k, _):
        expert = (ep + 16 + k) % EXPERTS

        @pl.when(jnp.logical_not((expert == ep) & own))
        def _():
            tell(place(expert, x_=home))

        return 0

    lax.fori_loop(0, EXPERTS, tell_expert, 0)

    def tell_groups(k, _):
        tell(at(z_=RING * k + 3))
        return 0

    def tell_group(k, _):
        tell(at(z_=RING * group + k))
        return 0

    lax.fori_loop(0, group, tell_groups, 0)
    lax.fori_loop(0, inner, tell_group, 0)
    for k in range(1, 16):
        tell(at(y_=(y + k // RING) % RING, x_=(x + k % RING) % RING))
    tell(at(c_=1 - c))

    for load in loads[:4]:
        load.wait()
    rows = rows_ref[...].astype(F32)
    scale = lax.rsqrt(jnp.mean(rows * rows, axis=-1, keepdims=True) + 1.0)
    xn[...] = (rows * scale * egain_ref[...]).astype(BF16)

    row_count = rows_ref.shape[0]
    slots = EXPERTS * CAP
    expert_at = iota((EXPERTS, row_count), 0)
    chosen = jnp.zeros((EXPERTS, row_count), F32)
    weight = jnp.zeros((EXPERTS, row_count), F32)
    for k in range(4):
        hit = idx_ref[k : k + 1, :] == expert_at
        chosen = jnp.where(hit, 1.0, chosen)
        weight = jnp.where(hit, wgt_ref[k : k + 1, :], weight)
    earlier = iota((row_count, row_count), 0) < iota((row_count, row_count), 1)
    rank = dot(chosen.astype(BF16), earlier.astype(F32).astype(BF16))
    label = jnp.where(chosen > 0.0, rank, -1.0).astype(BF16)
    slot_s, slot_e = iota((slots, EXPERTS), 0), iota((slots, EXPERTS), 1)
    spread = ((slot_s >= slot_e * CAP) & (slot_s < slot_e * CAP + CAP)).astype(F32)
    within = jnp.sum(spread * (slot_s - slot_e * CAP).astype(F32), axis=1, keepdims=True)
    spread = spread.astype(BF16)
    placed = (dot(spread, label) == within).astype(F32)
    w_hi, w_lo = halves(weight)
    q_hi[...] = (placed * dot(spread, w_hi)).astype(BF16)
    q_lo[...] = (placed * dot(spread, w_lo)).astype(BF16)
    onehot[...] = placed.astype(BF16)

    @pl.when(own)
    def _():
        features = xn[:, pl.ds(pl.multiple_of(512 * y, 512), 512)]
        packed = dot(onehot[...], features)
        sbuf[...] = packed.reshape(EXPERTS, CAP, 512).astype(BF16)
        rbuf[y, ep // RING] = sbuf[ep]

    for load in loads[10:14]:
        load.wait()

    pl.semaphore_wait(barrier, 15 + 1 + (3 - inner) + jnp.where(last, later, 0) + 31 * mine + 32 - mine)

    def dispatch(e):
        return copy_to(
            sbuf.at[e], rbuf.at[y, ep // RING], dsp_s.at[0], dsp_r.at[ep // RING], place(e)
        )

    @pl.when(own)
    def _():
        dispatch((ep + 16) % EXPERTS).start()

        def send(k, _):
            dispatch((ep + 16 - k) % EXPERTS).start()
            dispatch((ep + 16 + k) % EXPERTS).start()
            return 0

        lax.fori_loop(1, 16, send, 0)

    def ring(piece, first_half, send_sem, recv_sem, p, axis):
        me = y if axis == "y" else x
        right, left, across = (me + 1) % RING, (me + 3) % RING, (me + 2) % RING

        def move(slot, way, to):
            device = at(y_=to) if axis == "y" else at(x_=to)
            return copy_to(piece(slot), piece(slot), send_sem, recv_sem.at[way, p], device)

        def start(way):
            move(me, way, left if way else right).start()

        def relay():
            if first_half:
                move(left, 0, right).wait_recv()
                move(left, 2, right).start()
            else:
                move(right, 1, left).wait_recv()
                move(right, 2, left).start()

        def near():
            if first_half:
                move(right, 1, left).wait_recv()
            else:
                move(left, 0, right).wait_recv()

        def far():
            move(across, 2, right).wait_recv()

        return start, relay, near, far

    weights = [
        ring(lambda s: gu.at[s, pl.ds(0, 64)], True, ws.at[0], wr, 0, "x"),
        ring(lambda s: gu.at[s, pl.ds(64, 64)], False, ws.at[0], wr, 1, "x"),
        ring(lambda s: wd.at[s, pl.ds(0, 512)], True, ws.at[1], wr, 2, "x"),
        ring(lambda s: wd.at[s, pl.ds(512, 512)], False, ws.at[1], wr, 3, "x"),
    ]
    row_ring, row_from = [], []
    for j, away in enumerate((4, 3, 5, 2, 6, 1, 7, 0)):
        k = (ep // RING + away) % SOURCES
        row_ring.append(ring(lambda s, k=k: rbuf.at[s, k], j % 2 == 0, ys.at[0], yr, j, "y"))
        row_from.append(k)
    hid_ring = [
        ring(lambda s: hid.at[s, pl.ds(0, 96)], True, hs.at[0], hr, 0, "y"),
        ring(lambda s: hid.at[s, pl.ds(96, 96)], False, hs.at[0], hr, 1, "y"),
    ]
    weights[0][0](0)
    weights[1][0](1)
    weights[1][0](0)
    weights[0][0](1)

    for load in loads[4:10]:
        load.wait()
    moves, sums = local_mixer(rec_ref, key_ref, val_ref, dec_ref, rate_ref, off_ref, xg, yf)
    cmap[0] = moves[:64] + pltpu.roll(sums[:64], 64, 1)
    cmap[1] = pltpu.roll(moves[64:], 64, 1) + sums[64:]
    swap = copy_to(cmap.at[1 - c], pmap, ps.at[0], pr.at[0], at(c_=1 - c))
    swap.start()

    pre = dot(cgu[...], xn[...], NT)
    shb[tp] = (silu(pre[:64]) * pre[64:]).astype(BF16)

    def share(k):
        return copy_to(
            shb.at[tp], shb.at[tp], sh_s.at[0], sh_r.at[0], at(y_=k // RING, x_=k % RING)
        )

    def share_send(k, _):
        share((tp + k) % 16).start()
        return 0

    lax.fori_loop(1, 16, share_send, 0)

    swap.wait_recv()
    lane = iota((64, 128), 1)
    first = jnp.where(c == 0, cmap[0], pmap[...])
    second = jnp.where(c == 0, pmap[...], cmap[1])

    def compose(later, earlier):
        stacked = jnp.concatenate([earlier, jnp.zeros_like(earlier)], axis=0)
        moved = dot3(halves(jnp.where(lane < 64, later, 0.0)), halves(stacked))
        return moved + jnp.where(lane < 64, 0.0, later)

    zmine[...] = compose(second, first).astype(BF16)

    def to_group(k):
        return copy_to(zmine, zmap.at[inner], zs.at[k], zr.at[inner], at(z_=RING * group + k))

    def send_group(k, _):
        to_group(k).start()
        return 0

    lax.fori_loop(inner + 1, RING, send_group, 0)

    def forward_rows(j):
        k = row_from[j]

        @pl.when(RING * k + x != ep)
        def _():
            copy_to(
                rbuf.at[y, k], rbuf.at[y, k], dsp_s.at[0], dsp_r.at[k], place(RING * k + x)
            ).wait_recv()

        row_ring[j][0](0)
        row_ring[j][0](1)

    weights[0][1]()
    weights[1][1]()
    for j in range(4):
        forward_rows(j)
    def advance(step):
        step = step.astype(F32)
        low = jnp.where(lane < 64, step, 0.0)
        twice = (low + pltpu.roll(low, 64, 1)).astype(BF16)
        k_hi, k_lo = halves(keep[...])
        moved = dot(twice, jnp.concatenate([k_hi, k_lo], axis=0))
        keep[...] = moved + jnp.where(lane < 64, 0.0, step)

    def in_group(k, _):
        copy_to(zmine, zmap.at[k], zs.at[0], zr.at[k], at(z_=RING * group + k)).wait_recv()
        advance(zmap[k])
        return 0

    def to_later(k):
        return copy_to(zlast, zall.at[group], zls.at[0], zlr.at[group], at(z_=k))

    keep[...] = (iota((64, 128), 0) == lane).astype(F32)
    lax.fori_loop(0, inner, in_group, 0)
    ahead[...] = keep[...]

    @pl.when(last)
    def _():
        advance(zmine[...])
        zlast[...] = keep[...].astype(BF16)

        def send_later(k, _):
            to_later(k).start()
            return 0

        lax.fori_loop(RING * (group + 1), nz, send_later, 0)

    for j in range(4, 8):
        forward_rows(j)
    for ring_of in row_ring:
        ring_of[1]()
    for load in loads[14:]:
        load.wait()
    weights[2][0](0)
    weights[3][0](1)
    weights[3][0](0)
    weights[2][0](1)

    for part in (0, 1):
        weights[part][2]()
        weights[part][3]()

    def product(slot):
        taken = rbuf[slot].astype(F32).reshape(SOURCES * CAP, 512).astype(BF16)
        span = pl.ds(pl.multiple_of(512 * slot, 512), 512)
        g = gu[:, 0:64, span].reshape(256, 512)
        u = gu[:, 64:128, span].reshape(256, 512)
        return dot(taken, g, NT), dot(taken, u, NT)

    g0, u0 = product(y)
    for ring_of in row_ring:
        ring_of[2]()
    g1, u1 = product((y + 1) % RING)
    g2, u2 = product((y + 3) % RING)
    for ring_of in row_ring:
        ring_of[3]()
    g3, u3 = product((y + 2) % RING)
    hidden = silu((g0 + g1) + (g2 + g3)) * ((u0 + u1) + (u2 + u3))
    hid[y] = hidden.astype(BF16)
    hid_ring[0][0](0)
    hid_ring[1][0](1)
    hid_ring[1][0](0)
    hid_ring[0][0](1)
    weights[2][1]()
    weights[3][1]()

    def over_groups(k, _):
        copy_to(zlast, zall.at[k], zls.at[0], zlr.at[k], at(z_=RING * k + 3)).wait_recv()
        advance(zall[k])
        return 0

    keep[...] = jnp.zeros((64, 128), F32)
    lax.fori_loop(0, group, over_groups, 0)
    state = jnp.where(lane < 64, 0.0, compose(ahead[...], keep[...]))
    passed = jnp.where(lane < 64, 0.0, compose(first, state))
    sts[c] = jnp.where(c == 0, state, passed)
    keep[...] = jnp.where(c == 0, passed, state)
    hand = copy_to(keep, sts.at[c], ps.at[1], pr.at[1], at(c_=1 - c))
    hand.start()
    copy_to(keep, sts.at[1 - c], ps.at[1], pr.at[1], at(c_=1 - c)).wait_recv()

    start = jnp.concatenate([pltpu.roll(sts[0], 64, 1), sts[1]], axis=0)
    readout = dot3(halves(xg[...]), halves(start)) + yf[...]
    same_head = ((iota((128, 128), 0) >> 6) == (iota((128, 128), 1) >> 6)).astype(F32)
    mean_of = (same_head * (1.0 / HEAD)).astype(BF16)
    same_head = same_head.astype(BF16)
    centred = readout - dot_exact_right(readout, mean_of)
    variance = dot_exact_right(centred * centred, mean_of)
    key = key_ref[...].astype(F32)
    bonus = dot_exact_right(rec_ref[...].astype(F32) * key * self_ref[...], same_head)
    mixed = (
        centred * lax.rsqrt(variance + 1.0) * gain_ref[...] + bonus * val_ref[...].astype(F32)
    ) * gate_ref[...].astype(F32)
    mixed = mixed.astype(BF16)

    def reduce_along(n, axis, piece, half, got_half, got_piece):
        me = y if axis == "y" else x
        right, left, across = (me + 1) % RING, (me + 3) % RING, (me + 2) % RING

        def to(way):
            side = left if way else right
            return at(y_=side) if axis == "y" else at(x_=side)

        def far(way):
            return copy_to(
                half(across, way), got_half.at[way], rs_s.at[n], rs_h.at[n, way], to(way)
            )

        def near(way):
            block = piece(left if way else right)
            return copy_to(block, got_piece.at[way], rs_s.at[n], rs_p.at[n, way], to(way))

        def first():
            far(0).start()
            far(1).start()

        def second():
            for way in range(2):
                far(way).wait_recv()
                mine_half = half(left if way else right, way)
                mine_half[...] = (
                    mine_half[...].astype(F32) + got_half[way].astype(F32)
                ).astype(BF16)
                near(way).start()

        def third():
            near(0).wait_recv()
            near(1).wait_recv()
            own_block = piece(me)[...].astype(F32)
            return own_block + got_piece[0].astype(F32) + got_piece[1].astype(F32)

        return first, second, third

    x_first = reduce_along(
        0, "x", lambda t: pb0.at[t], lambda t, h: pb0.at[t, pl.ds(2 * h, 2)], gh0, gp0
    )
    y_first = reduce_along(
        1, "y", lambda t: pb1.at[t], lambda t, h: pb1.at[t, pl.ds(2 * h, 2)], gh1, gp1
    )
    y_then = reduce_along(
        2, "y", lambda t: qb0.at[t], lambda t, h: qb0.at[t, :, pl.ds(512 * h, 512)], gh2, gp2
    )
    x_then = reduce_along(
        3, "x", lambda t: qb1.at[t], lambda t, h: qb1.at[t, :, pl.ds(512 * h, 512)], gh3, gp3
    )

    for block in range(4):
        partial = dot(mixed[64 * block : 64 * block + 64], wout[...])
        partial = partial.reshape(4, 16, 2048).astype(BF16)
        pb1[block] = partial[:, :, 1024:]
        for side in range(4):
            pb0[side, block] = partial[side, :, :1024]
    x_first[0]()
    y_first[0]()
    hid_ring[0][1]()
    hid_ring[1][1]()

    weights[2][2]()
    weights[3][2]()
    weights[2][3]()
    weights[3][3]()
    for ring_of in hid_ring:
        ring_of[2]()
        ring_of[3]()
    def give_back(k, s):
        return copy_to(
            obuf.at[s, k],
            retb.at[ep],
            ret_s.at[0],
            ret_r.at[0],
            place(RING * k + x, x_=s),
        )

    every_hidden = jnp.concatenate([hid[part] for part in range(RING)], axis=1)

    def send_back(s, away):
        k = (ep // RING + away) % SOURCES

        @pl.when(jnp.logical_not((RING * k + x == ep) & (s == x)))
        def _():
            give_back(k, s).start()

    for s in range(RING):
        made = dot(every_hidden, wd[s])
        obuf[s] = made.reshape(SOURCES, CAP, 128).astype(BF16)
        for away in (4, 3, 5, 2):
            send_back(s, away)
    for away in (6, 1, 7, 0):
        for s in range(RING):
            send_back(s, away)

    @pl.when(own)
    def _():
        retb[ep] = obuf[x, ep // RING]

    x_first[1]()
    y_first[1]()
    qb0[...] = x_first[2]().astype(BF16)
    y_then[0]()
    qb1[...] = y_first[2]().astype(BF16)
    x_then[0]()
    y_then[1]()
    x_then[1]()
    res0[:, :1024] = y_then[2]().astype(BF16)
    res0[:, 1024:] = x_then[2]().astype(BF16)
    put0 = pltpu.make_async_copy(res0, out0, od.at[0])
    put0.start()

    def whole(ref, send_sem, recv_sem):
        return copy_to(ref, ref, send_sem, recv_sem, at(c_=1 - c))

    others = shb.at[pl.ds(0, 15)]
    whole(others, sh_s.at[0], sh_r.at[0]).wait_recv()
    shared = dot(shb[...].reshape(1024, 128), cd[...], TN)

    @pl.when(own)
    def _():
        whole(sbuf.at[pl.ds(0, EXPERTS - 1)], dsp_s.at[0], dsp_r.at[0]).wait_send()

    for sent, sem in (
        (others, sh_s.at[0]),
        (gu.at[pl.ds(0, 3)], ws.at[0]),
        (wd.at[pl.ds(0, 3)], ws.at[1]),
        (rbuf.at[pl.ds(0, 3)], ys.at[0]),
        (hid.at[pl.ds(0, 3)], hs.at[0]),
        (pb0.at[pl.ds(0, 3)], rs_s.at[0]),
        (pb1.at[pl.ds(0, 3)], rs_s.at[1]),
        (qb0.at[pl.ds(0, 3)], rs_s.at[2]),
        (qb1.at[pl.ds(0, 3)], rs_s.at[3]),
    ):
        whole(sent, sem, dsp_r.at[0]).wait_send()
    swap.wait_send()
    hand.wait_send()

    def group_sent(k, _):
        to_group(k).wait_send()
        return 0

    lax.fori_loop(inner + 1, RING, group_sent, 0)
    for k in range(RING - 1):
        @pl.when(last & (group == k))
        def _():
            maps = q_hi.at[pl.ds(0, 64 * (12 - 4 * k))]
            whole(maps, zls.at[0], zlr.at[0]).wait_send()

    @pl.when(own)
    def _():
        whole(retb.at[pl.ds(0, EXPERTS - 1)], ret_s.at[0], ret_r.at[0]).wait()

    @pl.when(jnp.logical_not(own))
    def _():
        whole(retb, ret_s.at[0], ret_r.at[0]).wait()

    copies = retb[...].astype(F32).reshape(slots, 128).astype(BF16)
    merged = dot(q_hi[...], copies, TN) + dot(q_lo[...], copies, TN) + shared
    res1[...] = merged.astype(BF16)
    put1 = pltpu.make_async_copy(res1, out1, od.at[1])
    put1.start()
    put0.wait()

    put1.wait()


def on_device(
    receptance,
    key_tensor,
    value_tensor,
    decay_data_input,
    correction_rate_input,
    mixer_output_gate,
    decay_channel_offset,
    head_norm_gain,
    self_key_weight,
    mixer_output_weight,
    second_batch_rows,
    routed_expert_index,
    routing_output_weight,
    expert_norm_gain,
    expert_gate_weight,
    expert_up_weight,
    expert_down_weight,
    common_expert_gate,
    common_expert_up,
    common_expert_down,
):
    hbm = pl.BlockSpec(memory_space=pl.ANY)
    dma = pltpu.SemaphoreType.DMA
    rows = receptance.shape[0]
    scratch = [
        *(pltpu.VMEM((rows, 128), BF16) for _ in range(6)),
        *(pltpu.VMEM((1, 128), F32) for _ in range(3)),
        pltpu.VMEM((128, 2048), BF16),
        pltpu.VMEM((4, 128), jnp.int32),
        pltpu.VMEM((4, 128), F32),
        pltpu.VMEM((1, 2048), F32),
        pltpu.VMEM((128, 2048), BF16),
        pltpu.VMEM((RING, 128, 2048), BF16),
        pltpu.VMEM((RING, 1024, 128), BF16),
        pltpu.VMEM((128, 2048), BF16),
        pltpu.VMEM((1024, 128), BF16),
        pltpu.VMEM((128, 2048), BF16),
        pltpu.VMEM((EXPERTS, CAP, 512), BF16),
        pltpu.VMEM((RING, SOURCES, CAP, 512), BF16),
        pltpu.VMEM((RING, SOURCES * CAP, 256), BF16),
        pltpu.VMEM((RING, SOURCES, CAP, 128), BF16),
        pltpu.VMEM((EXPERTS, CAP, 128), BF16),
        pltpu.VMEM((RING, RING, 16, 1024), BF16),
        pltpu.VMEM((RING, RING, 16, 1024), BF16),
        pltpu.VMEM((RING, 16, 1024), BF16),
        pltpu.VMEM((RING, 16, 1024), BF16),
        pltpu.VMEM((2, 2, 16, 1024), BF16),
        pltpu.VMEM((2, 2, 16, 1024), BF16),
        pltpu.VMEM((2, 16, 512), BF16),
        pltpu.VMEM((2, 16, 512), BF16),
        pltpu.VMEM((2, RING, 16, 1024), BF16),
        pltpu.VMEM((2, RING, 16, 1024), BF16),
        pltpu.VMEM((2, 16, 1024), BF16),
        pltpu.VMEM((2, 16, 1024), BF16),
        pltpu.VMEM((16, 64, 128), BF16),
        pltpu.VMEM((EXPERTS * CAP, 128), BF16),
        pltpu.VMEM((EXPERTS * CAP, 128), BF16),
        pltpu.VMEM((EXPERTS * CAP, 128), BF16),
        pltpu.VMEM((256, 128), F32),
        pltpu.VMEM((256, 128), F32),
        pltpu.VMEM((2, 64, 128), F32),
        pltpu.VMEM((64, 128), F32),
        pltpu.VMEM((64, 128), BF16),
        pltpu.VMEM((RING, 64, 128), BF16),
        pltpu.VMEM((64, 128), BF16),
        pltpu.VMEM((RING, 64, 128), BF16),
        pltpu.VMEM((2, 64, 128), F32),
        pltpu.VMEM((64, 128), F32),
        pltpu.VMEM((64, 128), F32),
        pltpu.VMEM((16, 2048), BF16),
        pltpu.VMEM((128, 128), BF16),
        dma((20,)),
        dma((1,)),
        dma((SOURCES,)),
        dma((1,)),
        dma((3, SOURCES)),
        dma((2,)),
        dma((3, 4)),
        dma((1,)),
        dma((3, 2)),
        dma((1,)),
        dma((1,)),
        dma((4,)),
        dma((4, 2)),
        dma((4, 2)),
        dma((1,)),
        dma((1,)),
        dma((RING,)),
        dma((RING,)),
        dma((1,)),
        dma((RING,)),
        dma((2,)),
        dma((2,)),
        dma((2,)),
    ]
    return pl.pallas_call(
        kernel,
        out_shape=(
            jax.ShapeDtypeStruct((16, 2048), BF16),
            jax.ShapeDtypeStruct((128, 128), BF16),
        ),
        in_specs=[hbm] * 20,
        out_specs=(hbm, hbm),
        scratch_shapes=scratch,
        compiler_params=pltpu.CompilerParams(
            collective_id=0, has_side_effects=True, vmem_limit_bytes=60 * 1024 * 1024
        ),
        name="mixer_and_experts",
    )(
        receptance,
        key_tensor,
        value_tensor,
        decay_data_input,
        correction_rate_input,
        mixer_output_gate,
        decay_channel_offset.reshape(1, 128),
        head_norm_gain.reshape(1, 128),
        self_key_weight.reshape(1, 128),
        mixer_output_weight,
        second_batch_rows,
        routed_expert_index.T,
        routing_output_weight.T,
        expert_norm_gain.reshape(1, 2048),
        expert_gate_weight,
        expert_up_weight,
        expert_down_weight,
        common_expert_gate,
        common_expert_up,
        common_expert_down,
    )


def solution(mesh):
    split = Mesh(mesh.devices.reshape(16, 2, 4, 4), ("z", "c", "y", "x"))
    in_specs = (
        P(EP, TP),
        P(EP, TP),
        P(EP, TP),
        P(EP, TP),
        P(EP, TP),
        P(EP, TP),
        P(TP),
        P(TP),
        P(TP),
        P(TP, None),
        P(EP, None),
        P(EP, None),
        P(EP, None),
        P(),
        P(EP, TP, None),
        P(EP, TP, None),
        P(EP, None, TP),
        P(TP, None),
        P(TP, None),
        P(None, TP),
    )
    out_specs = (P(EP + TP, None), P(EP, TP))
    return jax.shard_map(
        on_device, mesh=split, in_specs=in_specs, out_specs=out_specs, check_vma=False
    )
```

time: 87.4 us -> 71.1 us (0.81)
  the two profiles are of different devices: /device:TPU:6 before, /device:TPU:32 now
where the time goes in v2:
time: 71.1 us; the launch traced here: 70.9 us
  Pallas kernels  68.1 us (96%)
  local copies, waits for them, and re-layouts  2.1 us (3%)
    pallas_call x1, Pallas kernels, on_device(): pl.pallas_call(kernel, out_shape=(jax.ShapeDtypeStruct((16, 2048), BF16),...  68.1 us
    unnamed x4, local copies, waits for them, and re-layouts  2.1 us

profile of v2, /device:TPU:32, one launch (start us, length us, event | category | flops | bytes accessed | tf_op | source)
XLA Modules:
  0.0 70.9 jit_solution(18365179223613845906)
XLA Ops:
  0.6 68.1 %mixer_and_experts.1 = (bf16[16,2048]{1,0:T(8,128)(2,1)}, bf16[128,128]{1,0:T(8,128)(2,1)}) custom-call(bf16[256,128]{1,0:T(8,128)(2,1)} %refs_0_.1, bf16[256,128]{1,0:T(8,128)(2,1)} %refs_1_.1, bf16[256,128]{1,0:T(8,128)(2,1)} %refs_2_.1, bf16[256,128]{1,0:T(8,128)(2,1)} %refs_3_.1, bf16[256,128]{1,0:T(8,128)(2,1)} %refs_4_.1, bf16[256,128]{1,0:T(8,128)(2,1)} %refs_5_.1, ...), custom_call_target="tpu_custom_call" | custom-call | tf_op jit(solution)/shard_map/mixer_and_experts/pallas_call | solution.py:895
  68.8 0.0 copy-start
  68.8 1.5 %copy.24 = bf16[16,2048]{1,0:T(8,128)(2,1)} copy(bf16[16,2048]{1,0:T(8,128)(2,1)} %get-tuple-element.4) | data formatting | bytes 131072
  70.3 0.0 copy-done
  70.3 0.6 copy.25
Async XLA Ops:
  68.8 1.5 %copy-start = (bf16[128,128]{1,0:T(8,128)(2,1)S(1)}, bf16[128,128]{1,0:T(8,128)(2,1)}, u32[]{:S(2)}) copy-start(bf16[128,128]{1,0:T(8,128)(2,1)} %get-tuple-element.5) | copy-start | bytes 98308

commit v3 on v2

--- a/solution.py
+++ b/solution.py
@@ -247,9 +247,7 @@
         sts,
         keep,
         ahead,
-        res0,
-        res1,
-    ) = refs[22:75]
+    ) = refs[22:73]
     (
         ld,
         dsp_s,
@@ -271,10 +269,9 @@
         zr,
         zls,
         zlr,
-        od,
         ps,
         pr,
-    ) = refs[75:]
+    ) = refs[73:]
     z, c = lax.axis_index("z"), lax.axis_index("c")
     y, x = lax.axis_index("y"), lax.axis_index("x")
     nz = lax.axis_size("z")
@@ -296,6 +293,9 @@
 
     def place(e, y_=None, x_=None):
         return at(e // 2, e % 2, y_, x_)
+
+    def whole(ref, send_sem, recv_sem):
+        return copy_to(ref, ref, send_sem, recv_sem, at(c_=1 - c))
 
     loads = []
     for source, target in (
@@ -339,17 +339,6 @@
 
     lax.fori_loop(0, SOURCES, tell_source, 0)
 
-    def tell_expert(k, _):
-        expert = (ep + 16 + k) % EXPERTS
-
-        @pl.when(jnp.logical_not((expert == ep) & own))
-        def _():
-            tell(place(expert, x_=home))
-
-        return 0
-
-    lax.fori_loop(0, EXPERTS, tell_expert, 0)
-
     def tell_groups(k, _):
         tell(at(z_=RING * k + 3))
         return 0
@@ -402,7 +391,7 @@
     for load in loads[10:14]:
         load.wait()
 
-    pl.semaphore_wait(barrier, 15 + 1 + (3 - inner) + jnp.where(last, later, 0) + 31 * mine + 32 - mine)
+    pl.semaphore_wait(barrier, 15 + 1 + (3 - inner) + jnp.where(last, later, 0) + 31 * mine)
 
     def dispatch(e):
         return copy_to(
@@ -479,18 +468,23 @@
     swap.start()
 
     pre = dot(cgu[...], xn[...], NT)
-    shb[tp] = (silu(pre[:64]) * pre[64:]).astype(BF16)
-
-    def share(k):
-        return copy_to(
-            shb.at[tp], shb.at[tp], sh_s.at[0], sh_r.at[0], at(y_=k // RING, x_=k % RING)
-        )
-
-    def share_send(k, _):
-        share((tp + k) % 16).start()
-        return 0
-
-    lax.fori_loop(1, 16, share_send, 0)
+    shb[y, x] = (silu(pre[:64]) * pre[64:]).astype(BF16)
+    share_x = [
+        ring(lambda s: shb.at[y, s, pl.ds(0, 32)], True, sh_s.at[0], sh_r.at[0], 0, "x"),
+        ring(lambda s: shb.at[y, s, pl.ds(32, 32)], False, sh_s.at[0], sh_r.at[0], 1, "x"),
+    ]
+    share_y = [
+        ring(lambda s: shb.at[s, pl.ds(0, 2)], True, sh_s.at[1], sh_r.at[1], 0, "y"),
+        ring(lambda s: shb.at[s, pl.ds(2, 2)], False, sh_s.at[1], sh_r.at[1], 1, "y"),
+    ]
+
+    def start_both(pair):
+        pair[0][0](0)
+        pair[1][0](1)
+        pair[1][0](0)
+        pair[0][0](1)
+
+    start_both(share_x)
 
     swap.wait_recv()
     lane = iota((64, 128), 1)
@@ -560,10 +554,15 @@
 
         lax.fori_loop(RING * (group + 1), nz, send_later, 0)
 
+    share_x[0][1]()
+    share_x[1][1]()
     for j in range(4, 8):
         forward_rows(j)
     for ring_of in row_ring:
         ring_of[1]()
+    for ring_of in share_x:
+        ring_of[2]()
+        ring_of[3]()
     for load in loads[14:]:
         load.wait()
     weights[2][0](0)
@@ -596,8 +595,7 @@
     hid_ring[1][0](1)
     hid_ring[1][0](0)
     hid_ring[0][0](1)
-    weights[2][1]()
-    weights[3][1]()
+    start_both(share_y)
 
     def over_groups(k, _):
         copy_to(zlast, zall.at[k], zls.at[0], zlr.at[k], at(z_=RING * k + 3)).wait_recv()
@@ -612,6 +610,12 @@
     keep[...] = jnp.where(c == 0, passed, state)
     hand = copy_to(keep, sts.at[c], ps.at[1], pr.at[1], at(c_=1 - c))
     hand.start()
+    hid_ring[0][1]()
+    hid_ring[1][1]()
+    weights[2][1]()
+    weights[3][1]()
+    share_y[0][1]()
+    share_y[1][1]()
     copy_to(keep, sts.at[1 - c], ps.at[1], pr.at[1], at(c_=1 - c)).wait_recv()
 
     start = jnp.concatenate([pltpu.roll(sts[0], 64, 1), sts[1]], axis=0)
@@ -687,8 +691,6 @@
             pb0[side, block] = partial[side, :, :1024]
     x_first[0]()
     y_first[0]()
-    hid_ring[0][1]()
-    hid_ring[1][1]()
 
     weights[2][2]()
     weights[3][2]()
@@ -706,6 +708,8 @@
             place(RING * k + x, x_=s),
         )
 
+    x_first[1]()
+    y_first[1]()
     every_hidden = jnp.concatenate([hid[part] for part in range(RING)], axis=1)
 
     def send_back(s, away):
@@ -728,24 +732,18 @@
     def _():
         retb[ep] = obuf[x, ep // RING]
 
-    x_first[1]()
-    y_first[1]()
     qb0[...] = x_first[2]().astype(BF16)
     y_then[0]()
     qb1[...] = y_first[2]().astype(BF16)
     x_then[0]()
     y_then[1]()
     x_then[1]()
-    res0[:, :1024] = y_then[2]().astype(BF16)
-    res0[:, 1024:] = x_then[2]().astype(BF16)
-    put0 = pltpu.make_async_copy(res0, out0, od.at[0])
-    put0.start()
-
-    def whole(ref, send_sem, recv_sem):
-        return copy_to(ref, ref, send_sem, recv_sem, at(c_=1 - c))
-
-    others = shb.at[pl.ds(0, 15)]
-    whole(others, sh_s.at[0], sh_r.at[0]).wait_recv()
+    out0[:, :1024] = y_then[2]().astype(BF16)
+    out0[:, 1024:] = x_then[2]().astype(BF16)
+
+    for ring_of in share_y:
+        ring_of[2]()
+        ring_of[3]()
     shared = dot(shb[...].reshape(1024, 128), cd[...], TN)
 
     @pl.when(own)
@@ -753,7 +751,8 @@
         whole(sbuf.at[pl.ds(0, EXPERTS - 1)], dsp_s.at[0], dsp_r.at[0]).wait_send()
 
     for sent, sem in (
-        (others, sh_s.at[0]),
+        (shb.at[y, pl.ds(0, 3)], sh_s.at[0]),
+        (shb.at[pl.ds(0, 3)], sh_s.at[1]),
         (gu.at[pl.ds(0, 3)], ws.at[0]),
         (wd.at[pl.ds(0, 3)], ws.at[1]),
         (rbuf.at[pl.ds(0, 3)], ys.at[0]),
@@ -788,12 +787,7 @@
 
     copies = retb[...].astype(F32).reshape(slots, 128).astype(BF16)
     merged = dot(q_hi[...], copies, TN) + dot(q_lo[...], copies, TN) + shared
-    res1[...] = merged.astype(BF16)
-    put1 = pltpu.make_async_copy(res1, out1, od.at[1])
-    put1.start()
-    put0.wait()
-
-    put1.wait()
+    out1[...] = merged.astype(BF16)
 
 
 def on_device(
@@ -819,6 +813,7 @@
     common_expert_down,
 ):
     hbm = pl.BlockSpec(memory_space=pl.ANY)
+    vmem = pl.BlockSpec(memory_space=pltpu.VMEM)
     dma = pltpu.SemaphoreType.DMA
     rows = receptance.shape[0]
     scratch = [
@@ -851,7 +846,7 @@
         pltpu.VMEM((2, RING, 16, 1024), BF16),
         pltpu.VMEM((2, 16, 1024), BF16),
         pltpu.VMEM((2, 16, 1024), BF16),
-        pltpu.VMEM((16, 64, 128), BF16),
+        pltpu.VMEM((RING, RING, 64, 128), BF16),
         pltpu.VMEM((EXPERTS * CAP, 128), BF16),
         pltpu.VMEM((EXPERTS * CAP, 128), BF16),
         pltpu.VMEM((EXPERTS * CAP, 128), BF16),
@@ -866,8 +861,6 @@
         pltpu.VMEM((2, 64, 128), F32),
         pltpu.VMEM((64, 128), F32),
         pltpu.VMEM((64, 128), F32),
-        pltpu.VMEM((16, 2048), BF16),
-        pltpu.VMEM((128, 128), BF16),
         dma((20,)),
         dma((1,)),
         dma((SOURCES,)),
@@ -882,24 +875,23 @@
         dma((4,)),
         dma((4, 2)),
         dma((4, 2)),
-        dma((1,)),
-        dma((1,)),
+        dma((2,)),
+        dma((2, 3, 2)),
         dma((RING,)),
         dma((RING,)),
         dma((1,)),
         dma((RING,)),
         dma((2,)),
         dma((2,)),
-        dma((2,)),
     ]
     return pl.pallas_call(
         kernel,
         out_shape=(
-            jax.ShapeDtypeStruct((16, 2048), BF16),
-            jax.ShapeDtypeStruct((128, 128), BF16),
+            pltpu.VMEM((16, 2048), BF16),
+            pltpu.VMEM((128, 128), BF16),
         ),
         in_specs=[hbm] * 20,
-        out_specs=(hbm, hbm),
+        out_specs=(vmem, vmem),
         scratch_shapes=scratch,
         compiler_params=pltpu.CompilerParams(
             collective_id=0, has_side_effects=True, vmem_limit_bytes=60 * 1024 * 1024

time: 71.1 us -> 64.2 us (0.903)
  the two profiles are of different devices: /device:TPU:32 before, /device:TPU:6 now
where the time goes in v3:
time: 64.2 us; the launch traced here: 63.7 us
  Pallas kernels  61.8 us (96%)
  local copies, waits for them, and re-layouts  1.25 us (2%)
  between operations  0.65 us (1%)
    pallas_call x1, Pallas kernels, on_device(): pl.pallas_call(kernel, out_shape=(pltpu.VMEM((16, 2048), BF16), pltpu.VME...  61.8 us

profile of v3, /device:TPU:6, one launch (start us, length us, event | category | flops | bytes accessed | tf_op | source)
XLA Modules:
  0.0 63.7 jit_solution(6641000259477233568)
XLA Ops:
  0.6 61.8 %mixer_and_experts.1 = (bf16[16,2048]{1,0:T(8,128)(2,1)S(1)}, bf16[128,128]{1,0:T(8,128)(2,1)S(1)}) custom-call(bf16[256,128]{1,0:T(8,128)(2,1)} %refs_0_.1, bf16[256,128]{1,0:T(8,128)(2,1)} %refs_1_.1, bf16[256,128]{1,0:T(8,128)(2,1)} %refs_2_.1, bf16[256,128]{1,0:T(8,128)(2,1)} %refs_3_.1, bf16[256,128]{1,0:T(8,128)(2,1)} %refs_4_.1, ...), custom_call_target="tpu_custom_call" | custom-call | tf_op jit(solution)/shard_map/mixer_and_experts/pallas_call | solution.py:887
  62.5 0.6 copy.24
  63.1 0.6 copy.25

commit v4 on v3

--- a/solution.py
+++ b/solution.py
@@ -226,8 +226,6 @@
         qb1,
         gh0,
         gh1,
-        gh2,
-        gh3,
         gp0,
         gp1,
         gp2,
@@ -247,7 +245,7 @@
         sts,
         keep,
         ahead,
-    ) = refs[22:73]
+    ) = refs[22:71]
     (
         ld,
         dsp_s,
@@ -271,7 +269,7 @@
         zlr,
         ps,
         pr,
-    ) = refs[73:]
+    ) = refs[71:]
     z, c = lax.axis_index("z"), lax.axis_index("c")
     y, x = lax.axis_index("y"), lax.axis_index("x")
     nz = lax.axis_size("z")
@@ -281,7 +279,6 @@
     mine = jnp.where(own, 1, 0)
     group, inner = z // RING, z % RING
     last = inner == RING - 1
-    later = nz - RING * (group + 1)
 
     def at(z_=None, c_=None, y_=None, x_=None):
         return {
@@ -320,7 +317,9 @@
         (gain_in, gain_ref),
         (self_in, self_ref),
     ):
-        loads.append(pltpu.make_async_copy(source, target, ld.at[len(loads)]))
+        count = len(loads)
+        slot = count if count < 10 else 10 if count < 14 else 11 if count < 17 else count - 5
+        loads.append(pltpu.make_async_copy(source, target, ld.at[slot]))
         loads[-1].start()
 
     barrier = pltpu.get_barrier_semaphore()
@@ -339,26 +338,19 @@
 
     lax.fori_loop(0, SOURCES, tell_source, 0)
 
-    def tell_groups(k, _):
-        tell(at(z_=RING * k + 3))
-        return 0
-
     def tell_group(k, _):
         tell(at(z_=RING * group + k))
         return 0
 
-    lax.fori_loop(0, group, tell_groups, 0)
     lax.fori_loop(0, inner, tell_group, 0)
-    for k in range(1, 16):
-        tell(at(y_=(y + k // RING) % RING, x_=(x + k % RING) % RING))
+    for k in range(1, RING):
+        tell(at(x_=(x + k) % RING))
+    for k in (1, 3):
+        tell(at(y_=(y + k) % RING))
     tell(at(c_=1 - c))
 
-    for load in loads[:4]:
+    for load in loads[2:4]:
         load.wait()
-    rows = rows_ref[...].astype(F32)
-    scale = lax.rsqrt(jnp.mean(rows * rows, axis=-1, keepdims=True) + 1.0)
-    xn[...] = (rows * scale * egain_ref[...]).astype(BF16)
-
     row_count = rows_ref.shape[0]
     slots = EXPERTS * CAP
     expert_at = iota((EXPERTS, row_count), 0)
@@ -381,6 +373,12 @@
     q_lo[...] = (placed * dot(spread, w_lo)).astype(BF16)
     onehot[...] = placed.astype(BF16)
 
+    for load in loads[:2]:
+        load.wait()
+    rows = rows_ref[...].astype(F32)
+    scale = lax.rsqrt(jnp.mean(rows * rows, axis=-1, keepdims=True) + 1.0)
+    xn[...] = (rows * scale * egain_ref[...]).astype(BF16)
+
     @pl.when(own)
     def _():
         features = xn[:, pl.ds(pl.multiple_of(512 * y, 512), 512)]
@@ -388,10 +386,9 @@
         sbuf[...] = packed.reshape(EXPERTS, CAP, 512).astype(BF16)
         rbuf[y, ep // RING] = sbuf[ep]
 
-    for load in loads[10:14]:
-        load.wait()
-
-    pl.semaphore_wait(barrier, 15 + 1 + (3 - inner) + jnp.where(last, later, 0) + 31 * mine)
+    pltpu.make_async_copy(gu.at[pl.ds(0, 2)], gu.at[pl.ds(0, 2)], ld.at[10]).wait()
+
+    pl.semaphore_wait(barrier, 5 + 1 + (3 - inner) + 31 * mine)
 
     def dispatch(e):
         return copy_to(
@@ -451,8 +448,18 @@
         row_ring.append(ring(lambda s, k=k: rbuf.at[s, k], j % 2 == 0, ys.at[0], yr, j, "y"))
         row_from.append(k)
     hid_ring = [
-        ring(lambda s: hid.at[s, pl.ds(0, 96)], True, hs.at[0], hr, 0, "y"),
-        ring(lambda s: hid.at[s, pl.ds(96, 96)], False, hs.at[0], hr, 1, "y"),
+        [
+            ring(
+                lambda s, h=h, p=p: hid.at[h, s, pl.ds(48 * p, 48)],
+                p == 0,
+                hs.at[h],
+                hr.at[h],
+                p,
+                "y",
+            )
+            for p in range(2)
+        ]
+        for h in range(2)
     ]
     weights[0][0](0)
     weights[1][0](1)
@@ -510,11 +517,15 @@
     def forward_rows(j):
         k = row_from[j]
 
-        @pl.when(RING * k + x != ep)
-        def _():
+        def arrived():
             copy_to(
                 rbuf.at[y, k], rbuf.at[y, k], dsp_s.at[0], dsp_r.at[k], place(RING * k + x)
             ).wait_recv()
+
+        if j < SOURCES - 1:
+            arrived()
+        else:
+            pl.when(jnp.logical_not(own))(arrived)
 
         row_ring[j][0](0)
         row_ring[j][0](1)
@@ -554,48 +565,46 @@
 
         lax.fori_loop(RING * (group + 1), nz, send_later, 0)
 
-    share_x[0][1]()
-    share_x[1][1]()
     for j in range(4, 8):
         forward_rows(j)
-    for ring_of in row_ring:
-        ring_of[1]()
-    for ring_of in share_x:
-        ring_of[2]()
-        ring_of[3]()
-    for load in loads[14:]:
+    pltpu.make_async_copy(wd, wd, ld.at[11]).wait()
+    for load in loads[17:]:
         load.wait()
     weights[2][0](0)
     weights[3][0](1)
     weights[3][0](0)
     weights[2][0](1)
 
+    for ring_of in row_ring:
+        ring_of[1]()
+    share_x[0][1]()
+    share_x[1][1]()
     for part in (0, 1):
         weights[part][2]()
         weights[part][3]()
 
-    def product(slot):
-        taken = rbuf[slot].astype(F32).reshape(SOURCES * CAP, 512).astype(BF16)
+    def product(slot, h):
+        taken = [rbuf[slot, row_from[j]].astype(F32) for j in range(4 * h, 4 * h + 4)]
+        taken = jnp.concatenate(taken, axis=0).astype(BF16)
         span = pl.ds(pl.multiple_of(512 * slot, 512), 512)
         g = gu[:, 0:64, span].reshape(256, 512)
         u = gu[:, 64:128, span].reshape(256, 512)
         return dot(taken, g, NT), dot(taken, u, NT)
 
-    g0, u0 = product(y)
-    for ring_of in row_ring:
-        ring_of[2]()
-    g1, u1 = product((y + 1) % RING)
-    g2, u2 = product((y + 3) % RING)
-    for ring_of in row_ring:
-        ring_of[3]()
-    g3, u3 = product((y + 2) % RING)
-    hidden = silu((g0 + g1) + (g2 + g3)) * ((u0 + u1) + (u2 + u3))
-    hid[y] = hidden.astype(BF16)
-    hid_ring[0][0](0)
-    hid_ring[1][0](1)
-    hid_ring[1][0](0)
-    hid_ring[0][0](1)
-    start_both(share_y)
+    for h in range(2):
+        for ring_of in row_ring[4 * h : 4 * h + 4]:
+            ring_of[2]()
+            ring_of[3]()
+        g0, u0 = product(y, h)
+        g1, u1 = product((y + 1) % RING, h)
+        g2, u2 = product((y + 3) % RING, h)
+        g3, u3 = product((y + 2) % RING, h)
+        hidden = silu((g0 + g1) + (g2 + g3)) * ((u0 + u1) + (u2 + u3))
+        hid[h, y] = hidden.astype(BF16)
+        start_both(hid_ring[h])
+        if h == 0:
+            weights[2][1]()
+            weights[3][1]()
 
     def over_groups(k, _):
         copy_to(zlast, zall.at[k], zls.at[0], zlr.at[k], at(z_=RING * k + 3)).wait_recv()
@@ -610,12 +619,8 @@
     keep[...] = jnp.where(c == 0, passed, state)
     hand = copy_to(keep, sts.at[c], ps.at[1], pr.at[1], at(c_=1 - c))
     hand.start()
-    hid_ring[0][1]()
-    hid_ring[1][1]()
-    weights[2][1]()
-    weights[3][1]()
-    share_y[0][1]()
-    share_y[1][1]()
+    hid_ring[0][0][1]()
+    hid_ring[0][1][1]()
     copy_to(keep, sts.at[1 - c], ps.at[1], pr.at[1], at(c_=1 - c)).wait_recv()
 
     start = jnp.concatenate([pltpu.roll(sts[0], 64, 1), sts[1]], axis=0)
@@ -676,12 +681,26 @@
     y_first = reduce_along(
         1, "y", lambda t: pb1.at[t], lambda t, h: pb1.at[t, pl.ds(2 * h, 2)], gh1, gp1
     )
-    y_then = reduce_along(
-        2, "y", lambda t: qb0.at[t], lambda t, h: qb0.at[t, :, pl.ds(512 * h, 512)], gh2, gp2
-    )
-    x_then = reduce_along(
-        3, "x", lambda t: qb1.at[t], lambda t, h: qb1.at[t, :, pl.ds(512 * h, 512)], gh3, gp3
-    )
+    def spread_along(n, axis, blocks, got):
+        me = y if axis == "y" else x
+
+        def start():
+            for k in (2, 1, 3):
+                to = (me + k) % RING
+                device = at(y_=to) if axis == "y" else at(x_=to)
+                copy_to(blocks.at[to], got.at[k - 1], rs_s.at[n], rs_h.at[n, 0], device).start()
+
+        def finish():
+            whole(got, rs_s.at[n], rs_h.at[n, 0]).wait_recv()
+            total = blocks[me].astype(F32)
+            for k in range(3):
+                total = total + got[k].astype(F32)
+            return total
+
+        return start, finish
+
+    y_then = spread_along(2, "y", qb0, gp2)
+    x_then = spread_along(3, "x", qb1, gp3)
 
     for block in range(4):
         partial = dot(mixed[64 * block : 64 * block + 64], wout[...])
@@ -689,57 +708,60 @@
         pb1[block] = partial[:, :, 1024:]
         for side in range(4):
             pb0[side, block] = partial[side, :, :1024]
+    hid_ring[1][0][1]()
+    hid_ring[1][1][1]()
     x_first[0]()
     y_first[0]()
 
-    weights[2][2]()
-    weights[3][2]()
-    weights[2][3]()
-    weights[3][3]()
-    for ring_of in hid_ring:
-        ring_of[2]()
-        ring_of[3]()
-    def give_back(k, s):
+    for part in (2, 3):
+        weights[part][2]()
+        weights[part][3]()
+
+    def give_back(j, s):
         return copy_to(
-            obuf.at[s, k],
+            obuf.at[s, j],
             retb.at[ep],
             ret_s.at[0],
             ret_r.at[0],
-            place(RING * k + x, x_=s),
+            place(RING * row_from[j] + x, x_=s),
         )
+
+    def second_product(h):
+        for ring_of in hid_ring[h]:
+            ring_of[2]()
+            ring_of[3]()
+        hidden = jnp.concatenate([hid[h, part] for part in range(RING)], axis=1)
+        for s in range(RING):
+            made = dot(hidden, wd[s])
+            obuf[s, 4 * h : 4 * h + 4] = made.reshape(4, CAP, 128).astype(BF16)
+            for j in range(4 * h, 4 * h + 4):
+                back = give_back(j, s)
+                if j < SOURCES - 1:
+                    back.start()
+                else:
+                    pl.when(jnp.logical_not(own & (s == x)))(back.start)
+
+    second_product(0)
+    for ring_of in share_x:
+        ring_of[2]()
+        ring_of[3]()
+    second_product(1)
+    start_both(share_y)
+
+    @pl.when(own)
+    def _():
+        retb[ep] = obuf[x, SOURCES - 1]
 
     x_first[1]()
     y_first[1]()
-    every_hidden = jnp.concatenate([hid[part] for part in range(RING)], axis=1)
-
-    def send_back(s, away):
-        k = (ep // RING + away) % SOURCES
-
-        @pl.when(jnp.logical_not((RING * k + x == ep) & (s == x)))
-        def _():
-            give_back(k, s).start()
-
-    for s in range(RING):
-        made = dot(every_hidden, wd[s])
-        obuf[s] = made.reshape(SOURCES, CAP, 128).astype(BF16)
-        for away in (4, 3, 5, 2):
-            send_back(s, away)
-    for away in (6, 1, 7, 0):
-        for s in range(RING):
-            send_back(s, away)
-
-    @pl.when(own)
-    def _():
-        retb[ep] = obuf[x, ep // RING]
-
     qb0[...] = x_first[2]().astype(BF16)
     y_then[0]()
     qb1[...] = y_first[2]().astype(BF16)
     x_then[0]()
-    y_then[1]()
-    x_then[1]()
-    out0[:, :1024] = y_then[2]().astype(BF16)
-    out0[:, 1024:] = x_then[2]().astype(BF16)
+    share_y[0][1]()
+    share_y[1][1]()
+    out0[:, :1024] = y_then[1]().astype(BF16)
+    out0[:, 1024:] = x_then[1]().astype(BF16)
 
     for ring_of in share_y:
         ring_of[2]()
@@ -756,7 +778,8 @@
         (gu.at[pl.ds(0, 3)], ws.at[0]),
         (wd.at[pl.ds(0, 3)], ws.at[1]),
         (rbuf.at[pl.ds(0, 3)], ys.at[0]),
-        (hid.at[pl.ds(0, 3)], hs.at[0]),
+        (hid.at[0, pl.ds(0, 3)], hs.at[0]),
+        (hid.at[1, pl.ds(0, 3)], hs.at[1]),
         (pb0.at[pl.ds(0, 3)], rs_s.at[0]),
         (pb1.at[pl.ds(0, 3)], rs_s.at[1]),
         (qb0.at[pl.ds(0, 3)], rs_s.at[2]),
@@ -831,7 +854,7 @@
         pltpu.VMEM((128, 2048), BF16),
         pltpu.VMEM((EXPERTS, CAP, 512), BF16),
         pltpu.VMEM((RING, SOURCES, CAP, 512), BF16),
-        pltpu.VMEM((RING, SOURCES * CAP, 256), BF16),
+        pltpu.VMEM((2, RING, SOURCES * CAP // 2, 256), BF16),
         pltpu.VMEM((RING, SOURCES, CAP, 128), BF16),
         pltpu.VMEM((EXPERTS, CAP, 128), BF16),
         pltpu.VMEM((RING, RING, 16, 1024), BF16),
@@ -840,12 +863,10 @@
         pltpu.VMEM((RING, 16, 1024), BF16),
         pltpu.VMEM((2, 2, 16, 1024), BF16),
         pltpu.VMEM((2, 2, 16, 1024), BF16),
-        pltpu.VMEM((2, 16, 512), BF16),
-        pltpu.VMEM((2, 16, 512), BF16),
         pltpu.VMEM((2, RING, 16, 1024), BF16),
         pltpu.VMEM((2, RING, 16, 1024), BF16),
-        pltpu.VMEM((2, 16, 1024), BF16),
-        pltpu.VMEM((2, 16, 1024), BF16),
+        pltpu.VMEM((3, 16, 1024), BF16),
+        pltpu.VMEM((3, 16, 1024), BF16),
         pltpu.VMEM((RING, RING, 64, 128), BF16),
         pltpu.VMEM((EXPERTS * CAP, 128), BF16),
         pltpu.VMEM((EXPERTS * CAP, 128), BF16),
@@ -861,20 +882,20 @@
         pltpu.VMEM((2, 64, 128), F32),
         pltpu.VMEM((64, 128), F32),
         pltpu.VMEM((64, 128), F32),
-        dma((20,)),
+        dma((15,)),
         dma((1,)),
         dma((SOURCES,)),
         dma((1,)),
         dma((3, SOURCES)),
         dma((2,)),
         dma((3, 4)),
-        dma((1,)),
-        dma((3, 2)),
+        dma((2,)),
+        dma((2, 3, 2)),
         dma((1,)),
         dma((1,)),
         dma((4,)),
         dma((4, 2)),
-        dma((4, 2)),
+        dma((2, 2)),
         dma((2,)),
         dma((2, 3, 2)),
         dma((RING,)),

time: 64.2 us -> 61.1 us (0.952)
  Pallas kernels: 61.8 us -> 59.1 us
    pallas_call x1, Pallas kernels: 61.8 us -> 59.1 us  [on_device(): pl.pallas_call(kernel, out_shape=(pltpu.VMEM((16, 2048), BF16), pltpu.VME...]
where the time goes in v4:
time: 61.1 us; the launch traced here: 61 us
  Pallas kernels  59.1 us (97%)
  local copies, waits for them, and re-layouts  1.25 us (2%)
  between operations  0.65 us (1%)
    pallas_call x1, Pallas kernels, on_device(): pl.pallas_call(kernel, out_shape=(pltpu.VMEM((16, 2048), BF16), pltpu.VME...  59.1 us
    unnamed x2, local copies, waits for them, and re-layouts  1.25 us

profile of v4, /device:TPU:6, one launch (start us, length us, event | category | flops | bytes accessed | tf_op | source)
XLA Modules:
  0.0 61.0 jit_solution(12967945426987384785)
XLA Ops:
  0.6 59.1 %mixer_and_experts.1 = (bf16[16,2048]{1,0:T(8,128)(2,1)S(1)}, bf16[128,128]{1,0:T(8,128)(2,1)S(1)}) custom-call(bf16[256,128]{1,0:T(8,128)(2,1)} %refs_0_.1, bf16[256,128]{1,0:T(8,128)(2,1)} %refs_1_.1, bf16[256,128]{1,0:T(8,128)(2,1)} %refs_2_.1, bf16[256,128]{1,0:T(8,128)(2,1)} %refs_3_.1, bf16[256,128]{1,0:T(8,128)(2,1)} %refs_4_.1, ...), custom_call_target="tpu_custom_call" | custom-call | tf_op jit(solution)/shard_map/mixer_and_experts/pallas_call | solution.py:908
  59.7 0.6 %copy.24 = bf16[16,2048]{1,0:T(8,128)(2,1)} copy(bf16[16,2048]{1,0:T(8,128)(2,1)S(1)} %get-tuple-element.2) | data formatting | bytes 131072
  60.4 0.6 %copy.25 = bf16[128,128]{1,0:T(8,128)(2,1)} copy(bf16[128,128]{1,0:T(8,128)(2,1)S(1)} %get-tuple-element.3) | data formatting | bytes 65536

commit v5 on v4

--- a/solution.py
+++ b/solution.py
@@ -296,10 +296,10 @@
 
     loads = []
     for source, target in (
+        (idx_in, idx_ref),
+        (wgt_in, wgt_ref),
         (rows_in, rows_ref),
         (egain_in, egain_ref),
-        (idx_in, idx_ref),
-        (wgt_in, wgt_ref),
         (key_in, key_ref),
         (dec_in, dec_ref),
         (off_in, off_ref),
@@ -349,7 +349,7 @@
         tell(at(y_=(y + k) % RING))
     tell(at(c_=1 - c))
 
-    for load in loads[2:4]:
+    for load in loads[:2]:
         load.wait()
     row_count = rows_ref.shape[0]
     slots = EXPERTS * CAP
@@ -373,7 +373,7 @@
     q_lo[...] = (placed * dot(spread, w_lo)).astype(BF16)
     onehot[...] = placed.astype(BF16)
 
-    for load in loads[:2]:
+    for load in loads[2:4]:
         load.wait()
     rows = rows_ref[...].astype(F32)
     scale = lax.rsqrt(jnp.mean(rows * rows, axis=-1, keepdims=True) + 1.0)
@@ -406,13 +406,14 @@
 
         lax.fori_loop(1, 16, send, 0)
 
-    def ring(piece, first_half, send_sem, recv_sem, p, axis):
+    def ring(piece, first_half, send_sem, passed_on, rest, axis):
         me = y if axis == "y" else x
-        right, left, across = (me + 1) % RING, (me + 3) % RING, (me + 2) % RING
+        right, left = (me + 1) % RING, (me + 3) % RING
 
         def move(slot, way, to):
             device = at(y_=to) if axis == "y" else at(x_=to)
-            return copy_to(piece(slot), piece(slot), send_sem, recv_sem.at[way, p], device)
+            recv_sem = passed_on if way == (0 if first_half else 1) else rest
+            return copy_to(piece(slot), piece(slot), send_sem, recv_sem, device)
 
         def start(way):
             move(me, way, left if way else right).start()
@@ -425,27 +426,18 @@
                 move(right, 1, left).wait_recv()
                 move(right, 2, left).start()
 
-        def near():
-            if first_half:
-                move(right, 1, left).wait_recv()
-            else:
-                move(left, 0, right).wait_recv()
-
-        def far():
-            move(across, 2, right).wait_recv()
-
-        return start, relay, near, far
+        return start, relay
 
     weights = [
-        ring(lambda s: gu.at[s, pl.ds(0, 64)], True, ws.at[0], wr, 0, "x"),
-        ring(lambda s: gu.at[s, pl.ds(64, 64)], False, ws.at[0], wr, 1, "x"),
-        ring(lambda s: wd.at[s, pl.ds(0, 512)], True, ws.at[1], wr, 2, "x"),
-        ring(lambda s: wd.at[s, pl.ds(512, 512)], False, ws.at[1], wr, 3, "x"),
+        ring(lambda s: gu.at[s, pl.ds(0, 64)], True, ws.at[0], wr.at[0], wr.at[4], "x"),
+        ring(lambda s: gu.at[s, pl.ds(64, 64)], False, ws.at[0], wr.at[1], wr.at[4], "x"),
+        ring(lambda s: wd.at[s, pl.ds(0, 512)], True, ws.at[1], wr.at[2], wr.at[5], "x"),
+        ring(lambda s: wd.at[s, pl.ds(512, 512)], False, ws.at[1], wr.at[3], wr.at[5], "x"),
     ]
     row_ring, row_from = [], []
     for j, away in enumerate((4, 3, 5, 2, 6, 1, 7, 0)):
         k = (ep // RING + away) % SOURCES
-        row_ring.append(ring(lambda s, k=k: rbuf.at[s, k], j % 2 == 0, ys.at[0], yr, j, "y"))
+        row_ring.append(ring(lambda s, k=k: rbuf.at[s, k], j % 2 == 0, ys.at[0], yr.at[j], yr.at[8 + j // 4], "y"))
         row_from.append(k)
     hid_ring = [
         [
@@ -453,8 +445,8 @@
                 lambda s, h=h, p=p: hid.at[h, s, pl.ds(48 * p, 48)],
                 p == 0,
                 hs.at[h],
-                hr.at[h],
-                p,
+                hr.at[h, p],
+                hr.at[h, 2],
                 "y",
             )
             for p in range(2)
@@ -477,12 +469,12 @@
     pre = dot(cgu[...], xn[...], NT)
     shb[y, x] = (silu(pre[:64]) * pre[64:]).astype(BF16)
     share_x = [
-        ring(lambda s: shb.at[y, s, pl.ds(0, 32)], True, sh_s.at[0], sh_r.at[0], 0, "x"),
-        ring(lambda s: shb.at[y, s, pl.ds(32, 32)], False, sh_s.at[0], sh_r.at[0], 1, "x"),
+        ring(lambda s: shb.at[y, s, pl.ds(0, 32)], True, sh_s.at[0], sh_r.at[0, 0], sh_r.at[0, 2], "x"),
+        ring(lambda s: shb.at[y, s, pl.ds(32, 32)], False, sh_s.at[0], sh_r.at[0, 1], sh_r.at[0, 2], "x"),
     ]
     share_y = [
-        ring(lambda s: shb.at[s, pl.ds(0, 2)], True, sh_s.at[1], sh_r.at[1], 0, "y"),
-        ring(lambda s: shb.at[s, pl.ds(2, 2)], False, sh_s.at[1], sh_r.at[1], 1, "y"),
+        ring(lambda s: shb.at[s, pl.ds(0, 2)], True, sh_s.at[1], sh_r.at[1, 0], sh_r.at[1, 2], "y"),
+        ring(lambda s: shb.at[s, pl.ds(2, 2)], False, sh_s.at[1], sh_r.at[1, 1], sh_r.at[1, 2], "y"),
     ]
 
     def start_both(pair):
@@ -579,9 +571,7 @@
         ring_of[1]()
     share_x[0][1]()
     share_x[1][1]()
-    for part in (0, 1):
-        weights[part][2]()
-        weights[part][3]()
+    whole(gu.at[pl.ds(0, 2)], ws.at[0], wr.at[4]).wait_recv()
 
     def product(slot, h):
         taken = [rbuf[slot, row_from[j]].astype(F32) for j in range(4 * h, 4 * h + 4)]
@@ -592,9 +582,7 @@
         return dot(taken, g, NT), dot(taken, u, NT)
 
     for h in range(2):
-        for ring_of in row_ring[4 * h : 4 * h + 4]:
-            ring_of[2]()
-            ring_of[3]()
+        whole(rbuf.at[0], ys.at[0], yr.at[8 + h]).wait_recv()
         g0, u0 = product(y, h)
         g1, u1 = product((y + 1) % RING, h)
         g2, u2 = product((y + 3) % RING, h)
@@ -713,9 +701,7 @@
     x_first[0]()
     y_first[0]()
 
-    for part in (2, 3):
-        weights[part][2]()
-        weights[part][3]()
+    whole(wd.at[pl.ds(0, 2)], ws.at[1], wr.at[5]).wait_recv()
 
     def give_back(j, s):
         return copy_to(
@@ -727,9 +713,7 @@
         )
 
     def second_product(h):
-        for ring_of in hid_ring[h]:
-            ring_of[2]()
-            ring_of[3]()
+        whole(hid.at[h, pl.ds(0, 2)], hs.at[h], hr.at[h, 2]).wait_recv()
         hidden = jnp.concatenate([hid[h, part] for part in range(RING)], axis=1)
         for s in range(RING):
             made = dot(hidden, wd[s])
@@ -742,9 +726,7 @@
                     pl.when(jnp.logical_not(own & (s == x)))(back.start)
 
     second_product(0)
-    for ring_of in share_x:
-        ring_of[2]()
-        ring_of[3]()
+    whole(shb.at[y, pl.ds(0, 2)], sh_s.at[0], sh_r.at[0, 2]).wait_recv()
     second_product(1)
     start_both(share_y)
 
@@ -763,9 +745,7 @@
     out0[:, :1024] = y_then[1]().astype(BF16)
     out0[:, 1024:] = x_then[1]().astype(BF16)
 
-    for ring_of in share_y:
-        ring_of[2]()
-        ring_of[3]()
+    whole(shb.at[pl.ds(0, 2)], sh_s.at[1], sh_r.at[1, 2]).wait_recv()
     shared = dot(shb[...].reshape(1024, 128), cd[...], TN)
 
     @pl.when(own)
@@ -886,18 +866,18 @@
         dma((1,)),
         dma((SOURCES,)),
         dma((1,)),
-        dma((3, SOURCES)),
+        dma((SOURCES + 2,)),
         dma((2,)),
-        dma((3, 4)),
+        dma((6,)),
         dma((2,)),
-        dma((2, 3, 2)),
+        dma((2, 3)),
         dma((1,)),
         dma((1,)),
         dma((4,)),
         dma((4, 2)),
         dma((2, 2)),
         dma((2,)),
-        dma((2, 3, 2)),
+        dma((2, 3)),
         dma((RING,)),
         dma((RING,)),
         dma((1,)),

time: 61.1 us -> 60.8 us (level)
  no operation moved by 1% of the time
where the time goes in v5:
time: 60.8 us; the launch traced here: 60.7 us
  Pallas kernels  58.8 us (97%)
  local copies, waits for them, and re-layouts  1.25 us (2%)
  between operations  0.65 us (1%)
    pallas_call x1, Pallas kernels, on_device(): pl.pallas_call(kernel, out_shape=(pltpu.VMEM((16, 2048), BF16), pltpu.VME...  58.8 us
    unnamed x2, local copies, waits for them, and re-layouts  1.25 us

profile of v5, /device:TPU:6, one launch (start us, length us, event | category | flops | bytes accessed | tf_op | source)
XLA Modules:
  0.0 60.7 jit_solution(16636761686782648586)
XLA Ops:
  0.6 58.8 %mixer_and_experts.1 = (bf16[16,2048]{1,0:T(8,128)(2,1)S(1)}, bf16[128,128]{1,0:T(8,128)(2,1)S(1)}) custom-call(bf16[256,128]{1,0:T(8,128)(2,1)} %refs_0_.1, bf16[256,128]{1,0:T(8,128)(2,1)} %refs_1_.1, bf16[256,128]{1,0:T(8,128)(2,1)} %refs_2_.1, bf16[256,128]{1,0:T(8,128)(2,1)} %refs_3_.1, bf16[256,128]{1,0:T(8,128)(2,1)} %refs_4_.1, ...), custom_call_target="tpu_custom_call" | custom-call | tf_op jit(solution)/shard_map/mixer_and_experts/pallas_call | solution.py:888
  59.4 0.6 %copy.24 = bf16[16,2048]{1,0:T(8,128)(2,1)} copy(bf16[16,2048]{1,0:T(8,128)(2,1)S(1)} %get-tuple-element.2) | data formatting | bytes 131072
  60.1 0.6 %copy.25 = bf16[128,128]{1,0:T(8,128)(2,1)} copy(bf16[128,128]{1,0:T(8,128)(2,1)S(1)} %get-tuple-element.3) | data formatting | bytes 65536

commit v6 on v5

--- a/solution.py
+++ b/solution.py
@@ -611,6 +611,8 @@
     hid_ring[0][1][1]()
     copy_to(keep, sts.at[1 - c], ps.at[1], pr.at[1], at(c_=1 - c)).wait_recv()
 
+    hid_ring[1][0][1]()
+    hid_ring[1][1][1]()
     start = jnp.concatenate([pltpu.roll(sts[0], 64, 1), sts[1]], axis=0)
     readout = dot3(halves(xg[...]), halves(start)) + yf[...]
     same_head = ((iota((128, 128), 0) >> 6) == (iota((128, 128), 1) >> 6)).astype(F32)
@@ -696,8 +698,6 @@
         pb1[block] = partial[:, :, 1024:]
         for side in range(4):
             pb0[side, block] = partial[side, :, :1024]
-    hid_ring[1][0][1]()
-    hid_ring[1][1][1]()
     x_first[0]()
     y_first[0]()
 

time: 60.8 us -> 60.7 us (level)
  no operation moved by 1% of the time
where the time goes in v6:
time: 60.7 us; the launch traced here: 60.3 us
  Pallas kernels  58.4 us (96%)
  local copies, waits for them, and re-layouts  1.25 us (2%)
  between operations  0.65 us (1%)
    pallas_call x1, Pallas kernels, on_device(): pl.pallas_call(kernel, out_shape=(pltpu.VMEM((16, 2048), BF16), pltpu.VME...  58.4 us
    unnamed x2, local copies, waits for them, and re-layouts  1.25 us

profile of v6, /device:TPU:6, one launch (start us, length us, event | category | flops | bytes accessed | tf_op | source)
XLA Modules:
  0.0 60.3 jit_solution(18266580152147917874)
XLA Ops:
  0.6 58.4 %mixer_and_experts.1 = (bf16[16,2048]{1,0:T(8,128)(2,1)S(1)}, bf16[128,128]{1,0:T(8,128)(2,1)S(1)}) custom-call(bf16[256,128]{1,0:T(8,128)(2,1)} %refs_0_.1, bf16[256,128]{1,0:T(8,128)(2,1)} %refs_1_.1, bf16[256,128]{1,0:T(8,128)(2,1)} %refs_2_.1, bf16[256,128]{1,0:T(8,128)(2,1)} %refs_3_.1, bf16[256,128]{1,0:T(8,128)(2,1)} %refs_4_.1, ...), custom_call_target="tpu_custom_call" | custom-call | tf_op jit(solution)/shard_map/mixer_and_experts/pallas_call | solution.py:888
  59.1 0.6 %copy.24 = bf16[16,2048]{1,0:T(8,128)(2,1)} copy(bf16[16,2048]{1,0:T(8,128)(2,1)S(1)} %get-tuple-element.2) | data formatting | bytes 131072
  59.7 0.6 %copy.25 = bf16[128,128]{1,0:T(8,128)(2,1)} copy(bf16[128,128]{1,0:T(8,128)(2,1)S(1)} %get-tuple-element.3) | data formatting | bytes 65536
